TPU v7x, 32 devices: a whole 2x2x4 slice. The times are simulated.
32 devices in a mesh: grp: 2 (over y), dp: 2 (over x), kv: 4 (over z), tp: 2 (over core).
Axes of the slice: x: 2, y: 2, z: 4, core: 2. Of those that a mesh axis runs over, the one named last changes fastest.
Arguments:
- tokens: bfloat16 [256, 4, 4096], P(('grp', 'dp'), None, ('kv', 'tp')), parts along dimension 0, may hold values from -160 to 160
- norm_gain: float32 [4096], replicated, may hold values from 0.1 to 1.9
- w_query: bfloat16 [4096, 16, 64], P(None, 'kv'), may hold values from -0.09375 to 0.09375
- w_key: bfloat16 [4096, 16, 64], P(None, 'kv'), may hold values from -0.09375 to 0.09375
- w_value: bfloat16 [4096, 16, 128], P(None, 'kv', 'tp'), may hold values from -0.09375 to 0.09375
- w_outgate: bfloat16 [4096, 16, 128], P(None, 'kv', 'tp'), may hold values from -0.09375 to 0.09375
- w_input: bfloat16 [4096, 16], replicated, may hold values from -0.09375 to 0.09375
- w_forget: bfloat16 [4096, 16], replicated, may hold values from -0.09375 to 0.09375
- forget_bias: float32 [16], replicated, may hold values from -1 to 4
- head_gain: float32 [16, 128], replicated, may hold values from 0.1 to 1.9
- w_out: bfloat16 [16, 128, 4096], P('kv', 'tp'), may hold values from -0.125 to 0.125
- memory: float32 [256, 16, 128, 64], P(('grp', 'dp'), 'kv', 'tp'), parts along dimension 0, may hold values from -12 to 12
- normalizer: float32 [256, 16, 64], P(('grp', 'dp'), 'kv'), parts along dimension 0, may hold values from -12 to 12
- stabilizer: float32 [256, 16], P(('grp', 'dp'), 'kv'), parts along dimension 0, may hold values from -1 to 1
- prev_keys: bfloat16 [256, 4, 16, 64], P(('grp', 'dp'), None, 'kv'), parts along dimension 0, may hold values from -6 to 6
- prev_values: bfloat16 [256, 4, 16, 128], P(('grp', 'dp'), None, 'kv', 'tp'), parts along dimension 0, may hold values from -6 to 6
- prev_input: float32 [256, 4, 16], P(('grp', 'dp'), None, 'kv'), parts along dimension 0, may hold values from -4 to 4
- prev_forget: float32 [256, 4, 16], P(('grp', 'dp'), None, 'kv'), parts along dimension 0, may hold values from -2 to -0.02
- accepted: int32 [256], P(('grp', 'dp')), parts along dimension 0, may hold values from 0 to 4
Outputs:
- mixed: bfloat16 [256, 4, 4096], P(('grp', 'dp'), None, ('kv', 'tp')), parts along dimension 0
- new_memory: float32 [256, 16, 128, 64], P(('grp', 'dp'), 'kv', 'tp'), parts along dimension 0
- new_normalizer: float32 [256, 16, 64], P(('grp', 'dp'), 'kv'), parts along dimension 0
- new_stabilizer: float32 [256, 16], P(('grp', 'dp'), 'kv'), parts along dimension 0
- new_keys: bfloat16 [256, 4, 16, 64], P(('grp', 'dp'), None, 'kv'), parts along dimension 0
- new_values: bfloat16 [256, 4, 16, 128], P(('grp', 'dp'), None, 'kv', 'tp'), parts along dimension 0
- new_input: float32 [256, 4, 16], P(('grp', 'dp'), None, 'kv'), parts along dimension 0
- new_forget: float32 [256, 4, 16], P(('grp', 'dp'), None, 'kv'), parts along dimension 0
There are 2 independent parts, one for each index of `grp`. A program takes and returns all parts, laid end to end along the dimension named above; an argument that names none is the same for every part. Nothing has to cross between parts.
All inputs are finite; a program needn't handle non-finite values.
Results may differ from a plain program's by a relative error of at most 0.038.
Values may be sent and summed in bfloat16 or wider, within the bound.
A program may use at most 128 MiB of HBM per device.

v0:
```python
import jax
import jax.numpy as jnp
from jax import lax
from jax.sharding import PartitionSpec as P

EPS = 1e-06
FAR_NEGATIVE = -1e30
HIGHEST_PRECISION = lax.Precision.HIGHEST


def recurrent(
    query_f, key_all, value_all, gate_in, gate_forget, accepted, memory, normalizer, stabilizer
):
    proposals = query_f.shape[1]
    total_span = key_all.shape[1]
    position = jnp.arange(total_span, dtype=jnp.int32)
    dropped = (position[None, :] < proposals) & (position[None, :] >= accepted[:, None])
    forget = jnp.where(dropped[:, :, None], 0.0, gate_forget)
    inflow = jnp.where(dropped[:, :, None], FAR_NEGATIVE, gate_in)
    running = jnp.cumsum(forget, axis=1)
    latest = running[:, proposals:]
    spread = latest[:, :, None, :] - running[:, None, :, :] + inflow[:, None, :, :]
    causal = position[None, :] <= (proposals + jnp.arange(proposals, dtype=jnp.int32))[:, None]
    spread = jnp.where(causal[None, :, :, None], spread, FAR_NEGATIVE)
    carried = latest + stabilizer[:, None, :]
    ceiling = jnp.maximum(jnp.max(spread, axis=2), carried)
    scores = jnp.einsum("sthk,suhk->stuh", query_f, key_all, precision=HIGHEST_PRECISION)
    weights = jnp.exp(spread - ceiling[:, :, None, :]) * scores
    carry_scale = jnp.exp(carried - ceiling)
    numerator = jnp.einsum("stuh,suhv->sthv", weights, value_all, precision=HIGHEST_PRECISION)
    numerator = numerator + carry_scale[..., None] * jnp.einsum(
        "shvk,sthk->sthv", memory, query_f, precision=HIGHEST_PRECISION
    )
    denominator = jnp.sum(weights, axis=2) + carry_scale * jnp.einsum(
        "shk,sthk->sth", normalizer, query_f, precision=HIGHEST_PRECISION
    )
    cell_out = numerator / jnp.maximum(jnp.abs(denominator), jnp.exp(-ceiling))[..., None]
    boundary = running[:, proposals - 1]
    reached = boundary[:, None, :] - running[:, :proposals] + inflow[:, :proposals]
    new_stabilizer = jnp.maximum(boundary + stabilizer, jnp.max(reached, axis=1))
    decay_old = jnp.exp(boundary + stabilizer - new_stabilizer)
    shares = jnp.exp(reached - new_stabilizer[:, None, :])
    new_memory = decay_old[:, :, None, None] * memory + jnp.einsum(
        "sjh,sjhv,sjhk->shvk",
        shares,
        value_all[:, :proposals],
        key_all[:, :proposals],
        precision=HIGHEST_PRECISION,
    )
    new_normalizer = decay_old[:, :, None] * normalizer + jnp.einsum(
        "sjh,sjhk->shk", shares, key_all[:, :proposals], precision=HIGHEST_PRECISION
    )
    return (cell_out, new_memory, new_normalizer, new_stabilizer)


def shards(
    tokens,
    norm_gain,
    w_query,
    w_key,
    w_value,
    w_outgate,
    w_input,
    w_forget,
    forget_bias,
    head_gain,
    w_out,
    memory,
    normalizer,
    stabilizer,
    prev_keys,
    prev_values,
    prev_input,
    prev_forget,
    accepted,
):
    sequences, proposals, columns = tokens.shape
    model_width = w_query.shape[0]
    local_heads = w_query.shape[1]
    key_size = w_query.shape[2]
    value_part = w_value.shape[2]
    token_rows = sequences * proposals
    head_start = lax.axis_index("kv") * local_heads
    value_start = lax.axis_index("tp") * value_part
    input_cols = lax.dynamic_slice_in_dim(w_input, head_start, local_heads, 1)
    forget_cols = lax.dynamic_slice_in_dim(w_forget, head_start, local_heads, 1)
    forget_shift = lax.dynamic_slice_in_dim(forget_bias, head_start, local_heads, 0)
    gain_block = lax.dynamic_slice(head_gain, (head_start, value_start), (local_heads, value_part))
    gathered = lax.all_gather(tokens, ("kv", "tp"), axis=2, tiled=True)
    as_float = gathered.astype(jnp.float32)
    inv_scale = lax.rsqrt(jnp.mean(as_float * as_float, axis=-1, keepdims=True) + EPS)
    normed = (as_float * inv_scale * norm_gain).astype(jnp.bfloat16)
    normed = normed.reshape(token_rows, model_width)

    def project(weight):
        return jnp.dot(normed, weight.reshape(model_width, -1), preferred_element_type=jnp.float32)

    queries = (
        project(w_query).astype(jnp.bfloat16).reshape(sequences, proposals, local_heads, key_size)
    )
    new_keys = (
        project(w_key).astype(jnp.bfloat16).reshape(sequences, proposals, local_heads, key_size)
    )
    new_values = (
        project(w_value).astype(jnp.bfloat16).reshape(sequences, proposals, local_heads, value_part)
    )
    out_gate = project(w_outgate).reshape(sequences, proposals, local_heads, value_part)
    new_input = project(input_cols).reshape(sequences, proposals, local_heads)
    new_forget = jax.nn.log_sigmoid(
        project(forget_cols).reshape(sequences, proposals, local_heads) + forget_shift
    )
    query_f = queries.astype(jnp.float32) * key_size ** (-0.5)
    key_all = jnp.concatenate([prev_keys, new_keys], axis=1).astype(jnp.float32)
    value_all = jnp.concatenate([prev_values, new_values], axis=1).astype(jnp.float32)
    gate_in = jnp.concatenate([prev_input, new_input], axis=1)
    gate_forget = jnp.concatenate([prev_forget, new_forget], axis=1)
    cell_out, new_memory, new_normalizer, new_stabilizer = recurrent(
        query_f, key_all, value_all, gate_in, gate_forget, accepted, memory, normalizer, stabilizer
    )
    head_squares = lax.psum(jnp.sum(cell_out * cell_out, axis=-1), "tp")
    full_values = value_part * lax.axis_size("tp")
    inv_head = lax.rsqrt(head_squares / full_values + EPS)
    gated = (jax.nn.sigmoid(out_gate) * cell_out * inv_head[..., None] * gain_block).astype(
        jnp.bfloat16
    )
    flat_rows = gated.reshape(token_rows, local_heads * value_part)
    out_block = lax.all_to_all(
        w_out.reshape(1, local_heads * value_part, model_width),
        ("kv", "tp"),
        split_axis=2,
        concat_axis=0,
        tiled=True,
    )
    summed = jnp.einsum(
        "gtc,gcd->td",
        lax.all_gather(
            flat_rows.reshape(1, token_rows, local_heads * value_part),
            ("kv", "tp"),
            axis=0,
            tiled=True,
        ),
        out_block,
        preferred_element_type=jnp.float32,
    )
    mixed = summed.astype(jnp.bfloat16).reshape(sequences, proposals, out_block.shape[2])
    return (
        mixed,
        new_memory,
        new_normalizer,
        new_stabilizer,
        new_keys,
        new_values,
        new_input,
        new_forget,
    )


def solution(mesh):
    return jax.shard_map(
        shards,
        mesh=mesh,
        in_specs=(
            P(("grp", "dp"), None, ("kv", "tp")),
            P(),
            P(None, "kv", None),
            P(None, "kv", None),
            P(None, "kv", "tp"),
            P(None, "kv", "tp"),
            P(),
            P(),
            P(),
            P(),
            P("kv", "tp", None),
            P(("grp", "dp"), "kv", "tp", None),
            P(("grp", "dp"), "kv", None),
            P(("grp", "dp"), "kv"),
            P(("grp", "dp"), None, "kv", None),
            P(("grp", "dp"), None, "kv", "tp"),
            P(("grp", "dp"), None, "kv"),
            P(("grp", "dp"), None, "kv"),
            P(("grp", "dp")),
        ),
        out_specs=(
            P(("grp", "dp"), None, ("kv", "tp")),
            P(("grp", "dp"), "kv", "tp", None),
            P(("grp", "dp"), "kv", None),
            P(("grp", "dp"), "kv"),
            P(("grp", "dp"), None, "kv", None),
            P(("grp", "dp"), None, "kv", "tp"),
            P(("grp", "dp"), None, "kv"),
            P(("grp", "dp"), None, "kv"),
        ),
        check_vma=False,
    )
```

profile of v0, /device:TPU:0, one launch (start us, length us, event | category | flops | bytes accessed | tf_op | source)
XLA Modules:
  0.0 165.0 jit_solution(10992848654207811287)
XLA Ops:
  7.9 10.0 %copy.164 = bf16[1,256,4096]{1,0,2:T(2,128)(2,1)} copy(bf16[1,256,4096]{2,1,0:T(8,128)(2,1)} %bitcast.117) | data formatting | bytes 4194304 | tf_op jit(solution)/shard_map/reshape | solution.py:128
  18.4 22.9 %reduce = bf16[4096,256]{1,0:T(8,128)(2,1)} reduce(bf16[4096,1,256]{2,1,0:T(2,128)(2,1)} %bitcast.114, bf16[]{:T(256)} %broadcast.99), dimensions={1}, to_apply=%bitcast.96.reduce_sub_computation | reduce | bytes 4194306
  41.3 5.8 %reshape.176 = bf16[8,2,65536]{2,1,0:T(2,128)(2,1)} reshape(bf16[4096,256]{1,0:T(8,128)(2,1)} %reduce) | data formatting | bytes 4194304
  47.1 6.5 %all-to-all-start = ((bf16[8,2,65536]{2,1,0:T(2,128)(2,1)}), bf16[8,2,65536]{2,1,0:T(2,128)(2,1)}, u32[]{:S(2)}, u32[]{:S(2)}) async-start(bf16[8,2,65536]{2,1,0:T(2,128)(2,1)} %reshape.176), calls=%async_computation | async-start | bytes 4194304 | tf_op jit(solution)/shard_map/all_to_all | solution.py:127
  56.2 2.9 %fusion = f32[64,4]{1,0:T(8,128)S(1)} fusion(bf16[64,4,4096]{2,1,0:T(4,128)(2,1)} %all-gather.3.cloned.1.call-done), kind=kLoop, calls=%fused_computation.3 | loop fusion | flops 3145472 | bytes 2098176 | tf_op jit(solution)/shard_map/reduce_sum | solution.py:91
  59.1 1.9 %fusion.2 = bf16[64,4,4096]{2,1,0:T(4,128)(2,1)S(1)} fusion(bf16[64,4,4096]{2,1,0:T(4,128)(2,1)S(1)} %copy-done.1, f32[4096]{0:T(1024)S(1)} %copy-done.19, f32[64,4]{1,0:T(8,128)S(1)} %add_rsqrt_fusion), kind=kLoop, calls=%fused_computation.5 | loop fusion | flops 4194304 | bytes 4211712 | tf_op jit(solution)/shard_map/convert_element_type | solution.py:92
  62.4 3.2 %fusion.90 = f32[64,4,4]{0,2,1:T(4,128)S(1)} fusion(bf16[4096,16]{0,1:T(8,128)(2,1)} %param.26, s32[]{:T(128)S(6)} %select_n.29, bf16[64,4,4096]{2,1,0:T(4,128)(2,1)S(1)} %fusion.2, f32[4]{0:T(128)S(1)} %dynamic_slice.13), kind=kOutput, calls=%fused_computation.66 | convolution fusion | flops 8397824 | bytes 2134036 | tf_op jit(solution)/shard_map/dot_general | solution.py:96
  66.2 4.0 %reshape.159 = bf16[256,4096]{1,0:T(8,128)(2,1)} reshape(bf16[64,4,4096]{2,1,0:T(4,128)(2,1)} %copy-done.2) | data formatting | bytes 4194304 | tf_op jit(solution)/shard_map/reshape | solution.py:93
  70.3 3.9 %fusion.8 = f32[64,4,4]{0,2,1:T(4,128)S(1)} fusion(bf16[64,4,4096]{2,1,0:T(4,128)(2,1)} %copy-done.2, bf16[4096,16]{0,1:T(8,128)(2,1)} %param.25, s32[]{:T(128)S(6)} %select_n.29), kind=kOutput, calls=%fused_computation.11 | convolution fusion | flops 8388608 | bytes 2134020 | tf_op jit(solution)/shard_map/dot_general | solution.py:96
  77.3 2.3 %fusion.35 = f32[256,256]{1,0:T(8,128)S(1)} fusion(bf16[256,4096]{1,0:T(8,128)(2,1)} %reshape.159, bf16[4096,256]{0,1:T(8,128)(2,1)S(1)} %bitcast.113), kind=kOutput, calls=%fused_computation.24 | convolution fusion | flops 537067520 | bytes 4456448 | tf_op jit(solution)/shard_map/dot_general | solution.py:96
  79.8 3.6 %convolution_convert_fusion.1 = bf16[256,256]{1,0:T(8,128)(2,1)} fusion(bf16[256,4096]{1,0:T(8,128)(2,1)} %reshape.159, bf16[4096,256]{0,1:T(8,128)(2,1)} %bitcast.121), kind=kOutput, calls=%fused_computation.25 | convolution fusion | flops 536936448 | bytes 4325376 | tf_op jit(solution)/shard_map/dot_general | solution.py:96
  84.7 3.7 %convolution_convert_fusion.2 = bf16[256,256]{1,0:T(8,128)(2,1)} fusion(bf16[256,4096]{1,0:T(8,128)(2,1)} %reshape.159, bf16[4096,256]{0,1:T(8,128)(2,1)} %bitcast.122), kind=kOutput, calls=%fused_computation.26 | convolution fusion | flops 536936448 | bytes 4325376 | tf_op jit(solution)/shard_map/dot_general | solution.py:96
  88.4 3.1 %fusion.111 = (f32[64,4,4]{1,2,0:T(4,128)}, f32[64,4,8,4]{2,1,3,0:T(4,128)}) fusion(f32[64,4,4,64]{3,2,1,0:T(4,128)S(1)} %mul.94, bf16[64,4,4,64]{3,1,2,0:T(4,128)(2,1)S(1)} %copy.157, bf16[64,4,4,64]{3,1,2,0:T(4,128)(2,1)S(1)} %copy.156, f32[64,4,4]{1,2,0:T(4,128)S(1)} %copy-done.16, f32[64,8,4]{1,2,0:T(4,128)S(1)} %copy.153, f32[64,8,4]{1,2,0:T(4,128)S(1)} %copy.151, ...), kind=kOutput, calls=%fused_computation.95 | convolution fusion | flops 6863872 | bytes 585760 | tf_op jit(solution)/shard_map/sthk,suhk->stuh/dot_general | solution.py:27
  91.5 1.8 %fusion.80 = f32[64,4,1,4]{3,2,1,0:T(1,128)S(1)} fusion(f32[64,4,64,1]{2,3,1,0:T(1,128)S(1)} %bitcast.118, f32[64,4,4,64]{3,2,1,0:T(4,128)S(1)} %mul.94), kind=kOutput, calls=%fused_computation.51 | convolution fusion | flops 786432 | bytes 331776 | tf_op jit(solution)/shard_map/shk,sthk->sth/dot_general | solution.py:34
  96.4 2.4 %fusion.67 = f32[64,4,64,4]{2,3,1,0:T(4,128)S(1)} fusion(f32[64,4,8,4]{2,1,3,0:T(4,128)} %get-tuple-element.16, bf16[64,4,4,64]{3,1,2,0:T(4,128)(2,1)} %copy.148, bf16[64,4,4,64]{3,1,2,0:T(4,128)(2,1)} %copy.147), kind=kOutput, calls=%fused_computation.34 | convolution fusion | flops 6815744 | bytes 557056 | tf_op jit(solution)/shard_map/stuh,suhv->sthv/dot_general | solution.py:30
  98.9 15.6 %fusion.78 = f32[64,4,4,64]{3,2,1,0:T(4,128)S(1)} fusion(f32[64,4,64,64]{3,2,1,0:T(8,128)} %param.30, f32[64,4,4,64]{3,2,1,0:T(4,128)S(1)} %mul.94), kind=kOutput, calls=%fused_computation.49 | convolution fusion | flops 50331648 | bytes 4718592 | tf_op jit(solution)/shard_map/shvk,sthk->sthv/dot_general | solution.py:31
  115.9 2.6 %psum.7 = f32[64,4,4]{0,2,1:T(4,128)S(1)} all-reduce(f32[64,4,4]{0,2,1:T(4,128)S(1)} %multiply_reduce_fusion), channel_id=1, replica_groups=mesh['grp'=2,'dp'=2,'kv'=4,'tp'=2] {'tp'}, use_global_device_ids=true, to_apply=%region_5.6 | all-reduce | flops 1024 | bytes 8192 | tf_op jit(solution)/shard_map/psum | solution.py:120
  118.5 3.1 %fusion.126 = bf16[64,4,4096,1]{2,1,0,3:T(4,128)(2,1)S(1)} fusion(f32[4096]{0:T(1024)S(1)} %copy-done.20, f32[64,4]{1,0:T(8,128)S(1)} %copy-done.10, bf16[64,4,4096]{2,1,0:T(4,128)(2,1)} %all-gather.3.cloned.1.call-done), kind=kLoop, calls=%fused_computation.97 | loop fusion | flops 4194304 | bytes 4211712 | tf_op jit(solution)/shard_map/convert_element_type | solution.py:92
  121.7 2.1 %fusion.56 = bf16[64,4,4,64]{3,0,2,1:T(8,128)(2,1)S(1)} fusion(bf16[4096,4,64]{0,2,1:T(8,128)(2,1)S(1)} %copy-done.35, bf16[64,4,4096,1]{2,1,0,3:T(4,128)(2,1)S(1)} %fusion.126, f32[4,64]{1,0:T(4,128)S(1)} %copy-done.31, f32[64,4,4]{0,2,1:T(4,128)S(1)} %add_rsqrt_fusion.1, f32[64,4,4]{0,2,1:T(4,128)S(1)} %get-tuple-element.10, ...), kind=kOutput, calls=%fused_computation.31 | convolution fusion | flops 537526272 | bytes 4862976 | tf_op jit(solution)/shard_map/dot_general | solution.py:96
  125.0 7.0 %reshape.177 = bf16[4096,1,256]{2,1,0:T(2,128)(2,1)} reshape(bf16[8,2,65536]{2,1,0:T(2,128)(2,1)} %all-to-all-done) | data formatting | bytes 4194304
  132.0 3.9 %copy.178 = bf16[1,256,4096]{1,2,0:T(8,128)(2,1)} copy(bf16[1,256,4096]{1,0,2:T(2,128)(2,1)} %bitcast.115) | data formatting | bytes 4194304
  135.9 4.0 %copy.165 = bf16[1,256,8,512]{3,1,2,0:T(8,128)(2,1)} copy(bf16[1,256,8,512]{1,3,2,0:T(8,128)(2,1)} %bitcast.116) | data formatting | bytes 4194304 | tf_op jit(solution)/shard_map/all_to_all | solution.py:127
  142.4 12.3 %multiply_add_fusion = f32[64,4,64,64]{3,2,1,0:T(8,128)} fusion(f32[64,4,64,64]{3,2,1,0:T(8,128)} %param.30, f32[64,4]{1,0:T(8,128)S(1)} %copy.166, bf16[64,4,4,64]{3,1,2,0:T(4,128)(2,1)S(1)} %copy.156, f32[64,4,4,64]{3,2,1,0:T(4,128)S(1)} %convert_multiply_fusion.2), kind=kOutput, calls=%fused_computation | convolution fusion | flops 52428800 | bytes 8782848 | tf_op jit(solution)/shard_map/sjh,sjhv,sjhk->shvk/dot_general | solution.py:43
  154.7 2.6 %fusion.31 = bf16[256,512]{1,0:T(8,128)(2,1)S(1)} fusion(bf16[8,256,256]{2,1,0:T(8,128)(2,1)} %all-gather.5.cloned.1.call-done, bf16[1,256,8,512]{3,1,2,0:T(8,128)(2,1)} %copy.165), kind=kOutput, calls=%fused_computation.21 | convolution fusion | flops 537001984 | bytes 3407872 | tf_op jit(solution)/shard_map/gtc,gcd->td/dot_general | solution.py:134
  (122 shorter events, 19.0 us)
Async XLA Ops:
  7.2 70.1 %copy-start = (bf16[4096,4,64]{0,2,1:T(8,128)(2,1)S(1)}, bf16[4096,4,64]{0,2,1:T(8,128)(2,1)}, u32[]{:S(2)}) copy-start(bf16[4096,4,64]{0,2,1:T(8,128)(2,1)} %param.21) | copy-start | bytes 6291460
  7.2 49.0 %all-gather.3.cloned.1.call-start = ((), (), s32[]{:S(2)}) async-start(), calls=%async_computation.1 | async-start | bytes 2359296 | tf_op jit(solution)/shard_map/all_gather | solution.py:89
  47.1 6.6 %copy-start.11 = (bf16[64,4,4,64]{3,2,1,0:T(4,128)(2,1)S(1)}, bf16[64,4,4,64]{3,2,1,0:T(4,128)(2,1)}, u32[]{:S(2)}) copy-start(bf16[64,4,4,64]{3,2,1,0:T(4,128)(2,1)} %param.33) | copy-start | bytes 393220
  47.1 6.7 %copy-start.5 = (bf16[64,4,4,64]{3,2,1,0:T(4,128)(2,1)S(1)}, bf16[64,4,4,64]{3,2,1,0:T(4,128)(2,1)}, u32[]{:S(2)}) copy-start(bf16[64,4,4,64]{3,2,1,0:T(4,128)(2,1)} %param.34) | copy-start | bytes 393220
  47.1 7.5 %copy-start.36 = (f32[16]{0:T(128)S(1)}, f32[16]{0:T(128)}, u32[]{:S(2)}) copy-start(f32[16]{0:T(128)} %param.27) | copy-start | bytes 196
  47.1 9.0 %copy-start.34 = (s32[64]{0:T(128)S(1)}, s32[64]{0:T(128)}, u32[]{:S(2)}) copy-start(s32[64]{0:T(128)} %param.37) | copy-start | bytes 772
  47.1 77.9 %all-to-all-start = ((bf16[8,2,65536]{2,1,0:T(2,128)(2,1)}), bf16[8,2,65536]{2,1,0:T(2,128)(2,1)}, u32[]{:S(2)}, u32[]{:S(2)}) async-start(bf16[8,2,65536]{2,1,0:T(2,128)(2,1)} %reshape.176), calls=%async_computation | async-start | bytes 4194304 | tf_op jit(solution)/shard_map/all_to_all | solution.py:127
  53.6 5.5 %copy-start.19 = (f32[4096]{0:T(1024)S(1)}, f32[4096]{0:T(1024)}, u32[]{:S(2)}) copy-start(f32[4096]{0:T(1024)} %param.20) | copy-start | bytes 49156
  53.6 101.1 %all-gather.5.cloned.1.call-start = ((), (), s32[]{:S(2)}) async-start(), calls=%async_computation.2 | async-start | bytes 1179648 | tf_op jit(solution)/shard_map/all_gather | solution.py:136
  56.1 18.9 %copy-start.32 = (pred[4,8]{1,0:T(4,128)(4,1)}, pred[4,8]{1,0:T(4,128)(4,1)S(1)}, u32[]{:S(2)}) copy-start(pred[4,8]{1,0:T(4,128)(4,1)S(1)} %iota_compare_fusion.1) | copy-start | bytes 100
  66.2 9.7 %copy-start.23 = (f32[64,4]{0,1:T(4,128)}, f32[64,4]{0,1:T(4,128)S(1)}, u32[]{:S(2)}) copy-start(f32[64,4]{0,1:T(4,128)S(1)} %slice_bitcast_fusion) | copy-start | bytes 3076
  70.2 4.6 %copy-start.28 = (f32[64,4,4]{0,2,1:T(4,128)S(1)}, f32[64,4,4]{0,2,1:T(4,128)}, u32[]{:S(2)}) copy-start(f32[64,4,4]{0,2,1:T(4,128)} %param.35) | copy-start | bytes 12292
  70.2 5.7 %copy-start.21 = (f32[64,4]{0,1:T(4,128)S(1)}, f32[64,4]{0,1:T(4,128)}, u32[]{:S(2)}) copy-start(f32[64,4]{0,1:T(4,128)} %param.32) | copy-start | bytes 3076
  84.5 3.8 %copy-start.7 = (bf16[64,4,4,64]{3,2,1,0:T(4,128)(2,1)}, bf16[64,4,4,64]{3,2,1,0:T(4,128)(2,1)S(1)}, u32[]{:S(2)}) copy-start(bf16[64,4,4,64]{3,2,1,0:T(4,128)(2,1)S(1)} %reshape.163) | copy-start | bytes 393220
  91.4 4.9 %copy-start.22 = (f32[64,4]{0,1:T(4,128)S(1)}, f32[64,4]{0,1:T(4,128)}, u32[]{:S(2)}) copy-start(f32[64,4]{0,1:T(4,128)} %param.32) | copy-start | bytes 3076
  91.4 4.9 %copy-start.26 = (f32[64,4]{0,1:T(4,128)S(1)}, f32[64,4]{0,1:T(4,128)}, u32[]{:S(2)}) copy-start(f32[64,4]{0,1:T(4,128)} %get-tuple-element.13) | copy-start | bytes 3076
  91.4 4.9 %copy-start.13 = (f32[64,8,4]{0,2,1:T(4,128)S(1)}, f32[64,8,4]{0,2,1:T(4,128)}, u32[]{:S(2)}) copy-start(f32[64,8,4]{0,2,1:T(4,128)} %copy-done.12) | copy-start | bytes 24580
  91.4 4.9 %copy-start.18 = (f32[64,4,4]{0,2,1:T(4,128)S(1)}, f32[64,4,4]{0,2,1:T(4,128)}, u32[]{:S(2)}) copy-start(f32[64,4,4]{0,2,1:T(4,128)} %copy-done.17) | copy-start | bytes 12292
  91.4 4.9 %copy-start.24 = (f32[64,4]{0,1:T(4,128)S(1)}, f32[64,4]{0,1:T(4,128)}, u32[]{:S(2)}) copy-start(f32[64,4]{0,1:T(4,128)} %copy-done.23) | copy-start | bytes 3076
  96.3 18.1 %copy-start.25 = (f32[64,4]{0,1:T(4,128)}, f32[64,4]{0,1:T(4,128)S(1)}, u32[]{:S(2)}) copy-start(f32[64,4]{0,1:T(4,128)S(1)} %get-tuple-element.9) | copy-start | bytes 3076
  98.8 19.7 %copy-start.10 = (f32[64,4]{1,0:T(8,128)S(1)}, f32[64,4]{1,0:T(8,128)}, u32[]{:S(2)}) copy-start(f32[64,4]{1,0:T(8,128)} %copy-done.9) | copy-start | bytes 3076
  98.9 19.7 %copy-start.20 = (f32[4096]{0:T(1024)S(1)}, f32[4096]{0:T(1024)}, u32[]{:S(2)}) copy-start(f32[4096]{0:T(1024)} %param.20) | copy-start | bytes 49156
  135.9 5.3 %copy-start.15 = (f32[64,4,64]{2,1,0:T(4,128)S(1)}, f32[64,4,64]{2,1,0:T(4,128)}, u32[]{:S(2)}) copy-start(f32[64,4,64]{2,1,0:T(4,128)} %param.31) | copy-start | bytes 196612
  135.9 6.1 %copy-start.6 = (bf16[64,4,4,64]{3,2,1,0:T(4,128)(2,1)S(1)}, bf16[64,4,4,64]{3,2,1,0:T(4,128)(2,1)}, u32[]{:S(2)}) copy-start(bf16[64,4,4,64]{3,2,1,0:T(4,128)(2,1)} %param.34) | copy-start | bytes 393220
  (16 other events, 36.6 us)
Sparse Core Ops, SparseCore 0:
  9.6 33.3 all-gather.2
  125.1 23.5 all-gather.4
where the time goes:
time: 166 us; the launch traced here: 165 us
  matrix products  57.6 us (35%)
  local copies, waits for them, and re-layouts  48.6 us (29%)
  other arithmetic  34.2 us (21%)
  between operations  14.6 us (9%)
  starting transfers between devices  6.58 us (4%)
  blocking collectives  2.62 us (2%)
    unnamed x1, other arithmetic  22.9 us
    unnamed x80, local copies, waits for them, and re-layouts  21.5 us
    dot_general x6, matrix products, project(): jnp.dot(normed, weight.reshape(model_width, -1), preferred_element_type=j...  18.8 us
    dot_general x1, matrix products, recurrent(): jnp.einsum('shvk,sthk->sthv', memory, query_f, precision=HIGHEST_PRECISION)  15.6 us
    dot_general x1, matrix products, recurrent(): jnp.einsum('sjh,sjhv,sjhk->shvk', shares, value_all[:, :proposals], key_a...  12.3 us
    reshape x1, local copies, waits for them, and re-layouts, shards(): w_out.reshape(1, local_heads * value_part, model_width)  9.96 us
    all_to_all x1, starting transfers between devices, shards(): lax.all_to_all(w_out.reshape(1, local_heads * value_part, model_width), (...  6.5 us
    convert_element_type x2, other arithmetic, shards(): normed = (as_float * inv_scale * norm_gain).astype(jnp.bfloat16)  5.06 us
  transfers between devices with their start and end apart: 3, of which 0 were waited for; matrix products, arithmetic and copies ran while one was open for 81% of the time, Pallas kernels for 0%

commit v1 on v0

v1 whole, which is shorter than its diff:
```python
import functools
import jax
import jax.numpy as jnp
from jax import lax
from jax.sharding import PartitionSpec as P
from jax.experimental import pallas as pl
from jax.experimental.pallas import tpu as pltpu

EPS = 1e-06
FAR_NEGATIVE = -1e30
HIGHEST = lax.Precision.HIGHEST
MESH = pl.DeviceIdType.MESH
F32 = jnp.float32
BF16 = jnp.bfloat16
VMEM_LIMIT = 60 << 20


def nn(a, b, precision=None):
    return lax.dot_general(
        a, b, (((1,), (0,)), ((), ())), precision=precision, preferred_element_type=F32
    )


def nt(a, b, precision=None):
    return lax.dot_general(
        a, b, (((1,), (1,)), ((), ())), precision=precision, preferred_element_type=F32
    )


def enter(n, z, c):
    barrier = pltpu.get_barrier_semaphore()
    pl.semaphore_signal(barrier, inc=1, device_id={"tp": 1 - c}, device_id_type=MESH)

    @pl.when(z > 0)
    def _():
        pl.semaphore_signal(barrier, inc=1, device_id={"kv": z - 1}, device_id_type=MESH)

    @pl.when(z < n - 1)
    def _():
        pl.semaphore_signal(barrier, inc=1, device_id={"kv": z + 1}, device_id_type=MESH)

    peers = 1 + (z > 0).astype(jnp.int32) + (z < n - 1).astype(jnp.int32)
    pl.semaphore_wait(barrier, peers)


def project_kernel(
    n, key_size,
    x_ref, gain_ref, wq_hbm, wk_hbm, wv_hbm, wo_hbm, wi_ref, wf_ref, bias_ref, out_hbm,
    q_out, k_out, v_out, og_out, gi_out, gf_out, wout_out,
    xg, wq, wk, wv, wo, q_acc, k_acc, v_acc, o_acc, gi_acc, gf_acc, ssr_acc, ssc_acc,
    load_sem, send_sem, recv_sem, wsend_sem, wrecv_sem,
):
    z = lax.axis_index("kv")
    c = lax.axis_index("tp")
    width = x_ref.shape[1]
    loads = [
        pltpu.make_async_copy(src, dst, load_sem.at[i])
        for i, (src, dst) in enumerate(((wq_hbm, wq), (wk_hbm, wk), (wv_hbm, wv), (wo_hbm, wo)))
    ]
    for load in loads:
        load.start()
    enter(n, z, c)
    mine = 2 * z + c

    def hop(src, slot, way, target):
        return pltpu.make_async_remote_copy(
            src_ref=src, dst_ref=xg.at[slot],
            send_sem=send_sem.at[way, slot], recv_sem=recv_sem.at[slot],
            device_id=target, device_id_type=MESH,
        )

    up, down, side = {"kv": z + 1}, {"kv": z - 1}, {"tp": 1 - c}

    @pl.when(z < n - 1)
    def _():
        hop(x_ref, mine, 0, up).start()

    @pl.when(z > 0)
    def _():
        hop(x_ref, mine, 1, down).start()

    hop(x_ref, mine, 2, side).start()

    rows_out = out_hbm.shape[0]

    def out_piece(i):
        col = pl.multiple_of((2 * i + 1 - c) * width, width)
        return pltpu.make_async_remote_copy(
            src_ref=out_hbm.at[:, pl.ds(col, width)],
            dst_ref=wout_out.at[i, pl.ds(rows_out, rows_out)],
            send_sem=wsend_sem.at[i], recv_sem=wrecv_sem.at[i],
            device_id=side, device_id_type=MESH,
        )

    def own_piece(i):
        col = pl.multiple_of((2 * i + c) * width, width)
        return pltpu.make_async_copy(
            out_hbm.at[:, pl.ds(col, width)], wout_out.at[i, pl.ds(0, rows_out)],
            load_sem.at[4 + i],
        )

    for i in range(n):
        out_piece(i).start()
        own_piece(i).start()

    for acc in (q_acc, k_acc, v_acc, o_acc, gi_acc, gf_acc, ssr_acc, ssc_acc):
        acc[...] = jnp.zeros_like(acc)
    for load in loads:
        load.wait()

    def process(src, slot):
        cols = pl.ds(pl.multiple_of(slot * width, width), width)
        x = src[...].astype(F32)
        xs = (x * gain_ref[:, cols]).astype(BF16)
        square = x * x
        high = square.astype(BF16)
        low = (square - high.astype(F32)).astype(BF16)
        ones_row = jnp.ones((8, width), BF16)
        ones_col = jnp.ones((k_acc.shape[1], width), BF16)
        ssr_acc[...] += nt(ones_row, high) + nt(ones_row, low)
        ssc_acc[...] += nt(high, ones_col) + nt(low, ones_col)
        q_acc[...] += nt(wq[:, cols], xs)
        k_acc[...] += nt(xs, wk[:, cols])
        v_acc[...] += nt(wv[:, cols], xs)
        o_acc[...] += nt(wo[:, cols], xs)
        gi_acc[...] += nt(wi_ref[:, cols], xs)
        gf_acc[...] += nt(wf_ref[:, cols], xs)

    process(x_ref, mine)

    def partner_block(owner):
        slot = 2 * owner + 1 - c
        hop(x_ref, slot, 2, side).wait_recv()
        process(xg.at[slot], slot)

    partner_block(z)

    def step(k, carry):
        @pl.when(z - k >= 0)
        def _():
            slot = 2 * (z - k) + c
            hop(x_ref, slot, 0, up).wait_recv()

            @pl.when(z < n - 1)
            def _():
                hop(xg.at[slot], slot, 0, up).start()

            hop(xg.at[slot], slot, 2, side).start()

        @pl.when(z + k <= n - 1)
        def _():
            slot = 2 * (z + k) + c
            hop(x_ref, slot, 1, down).wait_recv()

            @pl.when(z > 0)
            def _():
                hop(xg.at[slot], slot, 1, down).start()

            hop(xg.at[slot], slot, 2, side).start()

        @pl.when(z - k >= 0)
        def _():
            slot = 2 * (z - k) + c
            process(xg.at[slot], slot)
            partner_block(z - k)

        @pl.when(z + k <= n - 1)
        def _():
            slot = 2 * (z + k) + c
            process(xg.at[slot], slot)
            partner_block(z + k)

        return carry

    lax.fori_loop(1, n, step, 0)

    inv_row = lax.rsqrt(ssr_acc[0:1] / gain_ref.shape[1] + EPS)
    inv_col = lax.rsqrt(ssc_acc[...] / gain_ref.shape[1] + EPS)
    q_out[...] = ((q_acc[...] * inv_row).astype(BF16).astype(F32) * key_size ** (-0.5)).astype(BF16)
    k_out[...] = (k_acc[...] * inv_col).astype(BF16)
    v_out[...] = (v_acc[...] * inv_row).astype(BF16)
    og_out[...] = o_acc[...] * inv_row
    all_heads = gf_acc.shape[0]
    diagonal = lax.broadcasted_iota(jnp.int32, (all_heads, all_heads), 0) == (
        lax.broadcasted_iota(jnp.int32, (all_heads, all_heads), 1)
    )
    shift = nn(jnp.where(diagonal, bias_ref[...], 0.0), jnp.ones(gf_acc.shape, F32), HIGHEST)
    gi_acc[...] = gi_acc[...] * inv_row
    raw = gf_acc[...] * inv_row + shift
    gf_acc[...] = jnp.minimum(raw, 0.0) - jnp.log1p(jnp.exp(-jnp.abs(raw)))
    local_heads = gi_out.shape[0]
    for acc, out in ((gi_acc, gi_out), (gf_acc, gf_out)):
        total = acc[:local_heads]
        for i in range(1, n):
            total = jnp.where(z == i, acc[i * local_heads : (i + 1) * local_heads], total)
        out[...] = total

    for i in range(n):
        own_piece(i).wait()
        out_piece(i).wait()

    def drain(i, carry):
        slot = 2 * i + c

        @pl.when((i <= z) & (z < n - 1))
        def _():
            hop(x_ref, slot, 0, up).wait_send()

        @pl.when((i >= z) & (z > 0))
        def _():
            hop(x_ref, slot, 1, down).wait_send()

        hop(x_ref, slot, 2, side).wait_send()
        return carry

    lax.fori_loop(0, n, drain, 0)


def recurrent_kernel(
    q_ref, k_ref, v_ref, og_ref, gi_ref, gf_ref, pk_ref, pv_ref, pi_ref, pf_ref,
    acc_ref, stab_ref, nrm_ref, gain_ref, mem_ref,
    nm_ref, nn_ref, ns_ref, ni_ref, nf_ref, g_ref, sq_ref,
    vts, kps, dfull, wexp, ro,
):
    step = pl.program_id(0)
    steps = pl.num_programs(0)
    block, heads, values, keys = mem_ref.shape
    span, _, seqs = pi_ref.shape
    rows = seqs * span
    lanes = 128
    iota = lambda shape, d: lax.broadcasted_iota(jnp.int32, shape, d)

    @pl.when(step == 0)
    def _():
        spread = (iota((seqs, rows), 0) == iota((seqs, rows), 1) // span)
        expand = spread.astype(F32)
        lane_pos = iota((span, rows), 1) % span == iota((span, rows), 0)
        eye = iota((seqs, seqs), 0) == iota((seqs, seqs), 1)
        dropped = iota((span, seqs), 0) >= acc_ref[...]
        ro[...] = jnp.zeros_like(ro)
        for h in range(heads):
            stab = stab_ref[h : h + 1, :]
            f = jnp.where(dropped, 0.0, pf_ref[:, h, :])
            i = jnp.where(dropped, FAR_NEGATIVE, pi_ref[:, h, :])
            new_i = nt(jnp.where(lane_pos, gi_ref[h : h + 1, :], 0.0), expand, HIGHEST)
            new_f = nt(jnp.where(lane_pos, gf_ref[h : h + 1, :], 0.0), expand, HIGHEST)
            ni_ref[:, h, :] = new_i
            nf_ref[:, h, :] = new_f
            total = []
            for j in range(span):
                total.append(f[j : j + 1] + total[-1] if total else f[0:1])
            e = total[-1]
            for j in range(span):
                total.append(total[-1] + new_f[j : j + 1])
            run_prev = jnp.concatenate(total[:span], axis=0)
            run_all = jnp.concatenate(total, axis=0)
            in_all = jnp.concatenate([i, new_i], axis=0)
            u = e - run_prev + i
            ns = jnp.maximum(e + stab, jnp.max(u, axis=0, keepdims=True))
            ns_ref[h : h + 1, :] = ns
            decay = jnp.exp(e + stab - ns)
            shares = jnp.exp(u - ns)
            share_row = jnp.sum(
                jnp.where(lane_pos, nn(shares, expand, HIGHEST), 0.0), axis=0, keepdims=True
            )
            kps[h] = pk_ref[:, h * keys : (h + 1) * keys]
            part = slice(h * values, (h + 1) * values)
            vts[part, :] = (pv_ref[part, :].astype(F32) * share_row).astype(BF16)
            full = nn(jnp.where(eye, decay, 0.0), jnp.ones((seqs, keys), F32), HIGHEST)
            dfull[h] = full
            mixed = jnp.where(spread, share_row, 0.0).astype(BF16)
            nn_ref[:, h, :] = full * nrm_ref[:, h, :] + nn(mixed, kps[h])
            gathered = jnp.zeros((16, rows), F32)
            position = iota((2 * span, seqs), 0)
            for t in range(span):
                latest = total[span + t]
                d = jnp.where(position <= span + t, latest - run_all + in_all, FAR_NEGATIVE)
                g = latest + stab
                top = jnp.maximum(jnp.max(d, axis=0, keepdims=True), g)
                pad = jnp.zeros((16 - 2 * span - 2, seqs), F32)
                stack = jnp.concatenate(
                    [jnp.exp(d - top), jnp.exp(g - top), jnp.exp(-top), pad], axis=0
                )
                wide = nn(stack, expand, HIGHEST)
                gathered = jnp.where(iota((16, rows), 1) % span == t, wide, gathered)
            wexp[h] = gathered

    first = step * block
    start = pl.multiple_of((first * span) // lanes * lanes, lanes)
    half = pl.ds(start, lanes)
    seq = (iota((values, lanes), 1) + start) // span - first
    for h in range(heads):
        part = slice(h * values, (h + 1) * values)
        memory = [mem_ref[s, h] for s in range(block)]
        packed = jnp.concatenate([m.astype(BF16) for m in memory], axis=0)
        read = nn(packed, q_ref[h * keys : (h + 1) * keys, half])
        total = ro[part, half]
        for s in range(block):
            total = jnp.where(seq == s, read[s * values : (s + 1) * values], total)
        ro[part, half] = total
        shared = vts[part, half]
        zero = jnp.zeros_like(shared)
        left = jnp.concatenate([jnp.where(seq == s, shared, zero) for s in range(block)], axis=0)
        update = nn(left, kps[h, half, :])
        for s in range(block):
            nm_ref[s, h] = (
                dfull[h, pl.ds(first + s, 1), :] * memory[s]
                + update[s * values : (s + 1) * values]
            )

    @pl.when(step == steps - 1)
    def _():
        same = iota((rows, rows), 0) // span == iota((rows, rows), 1) // span
        spread = iota((seqs, rows), 0) == iota((seqs, rows), 1) // span
        eye = iota((values, values), 0) == iota((values, values), 1)
        q = q_ref[...]
        owner = iota(q.shape, 0) // keys

        def tile(w):
            w = jnp.concatenate([w] * (8 // span), axis=0)
            return jnp.broadcast_to(w[None], (rows // 8, 8, rows)).reshape(rows, rows)

        for h in range(heads):
            part = slice(h * values, (h + 1) * values)
            only = jnp.where(owner == h, q, jnp.zeros_like(q))
            w = wexp[h]
            w_prev = jnp.where(same, tile(w[:span]) * nn(pk_ref[...], only), 0.0)
            w_new = jnp.where(same, tile(w[span : 2 * span]) * nn(k_ref[...], only), 0.0)
            carry = w[2 * span : 2 * span + 1]
            floor = w[2 * span + 1 : 2 * span + 2]
            top = nn(pv_ref[part, :], w_prev.astype(BF16)) + nn(v_ref[part, :], w_new.astype(BF16))
            top = top + carry * ro[part, :]
            nq = nn(nrm_ref[:, h, :].astype(BF16), q_ref[h * keys : (h + 1) * keys, :])
            nq = jnp.sum(jnp.where(spread, nq, 0.0), axis=0, keepdims=True)
            under = jnp.sum(w_prev + w_new, axis=0, keepdims=True) + carry * nq
            cell = top / jnp.maximum(jnp.abs(under), floor)
            sq_ref[h : h + 1, :] = jnp.sum(cell * cell, axis=0, keepdims=True)
            gain = nn(
                jnp.where(eye, gain_ref[h : h + 1, :], 0.0), jnp.ones((values, rows), F32), HIGHEST
            )
            g_ref[part, :] = (jax.nn.sigmoid(og_ref[part, :]) * cell * gain).astype(BF16)


def output_kernel(
    n, full_values,
    g_ref, sq_ref, w_ref,
    y_ref,
    g_in, sq_in, both, from_low, from_high, to_high, to_low,
    side_send, side_recv, up_send, up_recv, down_send, down_recv,
):
    z = lax.axis_index("kv")
    c = lax.axis_index("tp")
    enter(n, z, c)
    side = {"tp": 1 - c}
    swaps = [
        pltpu.make_async_remote_copy(
            src_ref=src, dst_ref=dst, send_sem=side_send.at[i], recv_sem=side_recv.at[i],
            device_id=side, device_id_type=MESH,
        )
        for i, (src, dst) in enumerate(((g_ref, g_in), (sq_ref, sq_in)))
    ]
    for swap in swaps:
        swap.start()
    for swap in swaps:
        swap.wait_recv()
    inv = lax.rsqrt((sq_ref[...] + sq_in[...]) / full_values + EPS)
    channels = g_ref.shape[0]
    heads = sq_ref.shape[0]
    values = channels // heads
    for i, src in enumerate((g_ref, g_in)):
        scaled = jnp.concatenate(
            [
                src[h * values : (h + 1) * values, :].astype(F32) * inv[h : h + 1, :]
                for h in range(heads)
            ],
            axis=0,
        )
        both[:, i * channels : (i + 1) * channels] = scaled.T.astype(BF16)

    def partial(d):
        return nn(both[...], w_ref[d])

    def upward(d):
        return pltpu.make_async_remote_copy(
            src_ref=to_high.at[d], dst_ref=from_low.at[d],
            send_sem=up_send.at[d], recv_sem=up_recv.at[d],
            device_id={"kv": z + 1}, device_id_type=MESH,
        )

    def downward(d):
        return pltpu.make_async_remote_copy(
            src_ref=to_low.at[d], dst_ref=from_high.at[d],
            send_sem=down_send.at[d], recv_sem=down_recv.at[d],
            device_id={"kv": z - 1}, device_id_type=MESH,
        )

    def step(i, carry):
        high = n - i
        low = i - 1

        @pl.when(high > z)
        def _():
            to_high[high] = partial(high).astype(BF16)

            @pl.when(z > 0)
            def _():
                upward(high).wait_recv()
                to_high[high] = (
                    to_high[high].astype(F32) + from_low[high].astype(F32)
                ).astype(BF16)

            upward(high).start()

        @pl.when(low < z)
        def _():
            to_low[low] = partial(low).astype(BF16)

            @pl.when(z < n - 1)
            def _():
                downward(low).wait_recv()
                to_low[low] = (
                    to_low[low].astype(F32) + from_high[low].astype(F32)
                ).astype(BF16)

            downward(low).start()

        return carry

    lax.fori_loop(1, n, step, 0)
    total = partial(z)
    y_ref[...] = total.astype(BF16)

    @pl.when(z == 0)
    def _():
        downward(z).wait_recv()
        y_ref[...] = (partial(z) + from_high[z].astype(F32)).astype(BF16)

    @pl.when(z == n - 1)
    def _():
        upward(z).wait_recv()
        y_ref[...] = (partial(z) + from_low[z].astype(F32)).astype(BF16)

    @pl.when((z > 0) & (z < n - 1))
    def _():
        upward(z).wait_recv()
        downward(z).wait_recv()
        y_ref[...] = (
            partial(z) + from_low[z].astype(F32) + from_high[z].astype(F32)
        ).astype(BF16)

    def drain(i, carry):
        @pl.when(n - i > z)
        def _():
            upward(n - i).wait_send()

        @pl.when(i - 1 < z)
        def _():
            downward(i - 1).wait_send()

        return carry

    lax.fori_loop(1, n, drain, 0)
    for swap in swaps:
        swap.wait_send()


def shards(
    n, tokens, norm_gain, w_query, w_key, w_value, w_outgate, w_input, w_forget, forget_bias,
    head_gain, w_out, memory, normalizer, stabilizer, prev_keys, prev_values, prev_input,
    prev_forget, accepted,
):
    seqs, span, width = tokens.shape
    depth, heads, keys = w_query.shape
    values = w_value.shape[2]
    rows = seqs * span
    hk, hv = heads * keys, heads * values
    all_heads = w_input.shape[1]
    sds = jax.ShapeDtypeStruct
    vm = pl.BlockSpec(memory_space=pltpu.VMEM)
    hbm = pl.BlockSpec(memory_space=pl.ANY)
    flip = lambda w: w.transpose(1, 2, 0).reshape(-1, depth)

    q, k, v, og, gi, gf, wout = pl.pallas_call(
        functools.partial(project_kernel, n, keys),
        out_shape=[
            sds((hk, rows), BF16), sds((rows, hk), BF16), sds((hv, rows), BF16),
            sds((hv, rows), F32), sds((heads, rows), F32), sds((heads, rows), F32),
            sds((n, 2 * hv, width), BF16),
        ],
        in_specs=[vm, vm, hbm, hbm, hbm, hbm, vm, vm, vm, hbm],
        out_specs=[vm] * 6 + [vm],
        scratch_shapes=[
            pltpu.VMEM((2 * n, rows, width), BF16),
            pltpu.VMEM((hk, depth), BF16), pltpu.VMEM((hk, depth), BF16),
            pltpu.VMEM((hv, depth), BF16), pltpu.VMEM((hv, depth), BF16),
            pltpu.VMEM((hk, rows), F32), pltpu.VMEM((rows, hk), F32),
            pltpu.VMEM((hv, rows), F32), pltpu.VMEM((hv, rows), F32),
            pltpu.VMEM((all_heads, rows), F32), pltpu.VMEM((all_heads, rows), F32),
            pltpu.VMEM((8, rows), F32), pltpu.VMEM((rows, hk), F32),
            pltpu.SemaphoreType.DMA((4 + n,)),
            pltpu.SemaphoreType.DMA((3, 2 * n)),
            pltpu.SemaphoreType.DMA((2 * n,)),
            pltpu.SemaphoreType.DMA((n,)),
            pltpu.SemaphoreType.DMA((n,)),
        ],
        compiler_params=pltpu.CompilerParams(
            collective_id=0, has_side_effects=True, vmem_limit_bytes=VMEM_LIMIT
        ),
        name="project",
    )(
        tokens.reshape(rows, width), norm_gain.reshape(1, depth),
        flip(w_query), flip(w_key), flip(w_value), flip(w_outgate),
        w_input.T, w_forget.T, forget_bias.reshape(1, all_heads), w_out.reshape(hv, -1),
    )

    gain_block = lax.dynamic_slice(
        head_gain,
        (lax.axis_index("kv") * heads, lax.axis_index("tp") * values),
        (heads, values),
    )
    block = 8
    whole = lambda *shape: pl.BlockSpec(shape, lambda i: (0,) * len(shape))
    tile = pl.BlockSpec((block, heads, values, keys), lambda i: (i, 0, 0, 0))
    new_memory, new_normalizer, ns, ni, nf, g, sq = pl.pallas_call(
        recurrent_kernel,
        grid=(seqs // block,),
        out_shape=[
            sds(memory.shape, F32), sds(normalizer.shape, F32), sds((heads, seqs), F32),
            sds((span, heads, seqs), F32), sds((span, heads, seqs), F32),
            sds((hv, rows), BF16), sds((heads, rows), F32),
        ],
        in_specs=[
            whole(hk, rows), whole(rows, hk), whole(hv, rows), whole(hv, rows),
            whole(heads, rows), whole(heads, rows), whole(rows, hk), whole(hv, rows),
            whole(span, heads, seqs), whole(span, heads, seqs), whole(1, seqs),
            whole(heads, seqs), whole(seqs, heads, keys), whole(heads, values), tile,
        ],
        out_specs=[
            tile, whole(seqs, heads, keys), whole(heads, seqs), whole(span, heads, seqs),
            whole(span, heads, seqs), whole(hv, rows), whole(heads, rows),
        ],
        scratch_shapes=[
            pltpu.VMEM((hv, rows), BF16), pltpu.VMEM((heads, rows, keys), BF16),
            pltpu.VMEM((heads, seqs, keys), F32), pltpu.VMEM((heads, 16, rows), F32),
            pltpu.VMEM((hv, rows), F32),
        ],
        compiler_params=pltpu.CompilerParams(vmem_limit_bytes=VMEM_LIMIT),
        name="recurrent",
    )(
        q, k, v, og, gi, gf, prev_keys.reshape(rows, hk),
        prev_values.reshape(rows, hv).T,
        prev_input.transpose(1, 2, 0), prev_forget.transpose(1, 2, 0),
        accepted.reshape(1, seqs), stabilizer.T, normalizer, gain_block, memory,
    )

    y = pl.pallas_call(
        functools.partial(output_kernel, n, values * 2),
        out_shape=sds((rows, width), BF16),
        in_specs=[vm] * 3,
        out_specs=vm,
        scratch_shapes=[
            pltpu.VMEM((hv, rows), BF16), pltpu.VMEM((heads, rows), F32),
            pltpu.VMEM((rows, 2 * hv), BF16),
            pltpu.VMEM((n, rows, width), BF16), pltpu.VMEM((n, rows, width), BF16),
            pltpu.VMEM((n, rows, width), BF16), pltpu.VMEM((n, rows, width), BF16),
            pltpu.SemaphoreType.DMA((2,)), pltpu.SemaphoreType.DMA((2,)),
            pltpu.SemaphoreType.DMA((n,)), pltpu.SemaphoreType.DMA((n,)),
            pltpu.SemaphoreType.DMA((n,)), pltpu.SemaphoreType.DMA((n,)),
        ],
        compiler_params=pltpu.CompilerParams(
            collective_id=1, has_side_effects=True, vmem_limit_bytes=VMEM_LIMIT
        ),
        name="output",
    )(g, sq, wout)

    return (
        y.reshape(seqs, span, width),
        new_memory,
        new_normalizer,
        ns.T,
        k.reshape(seqs, span, heads, keys),
        v.T.reshape(seqs, span, heads, values),
        ni.transpose(2, 0, 1),
        nf.transpose(2, 0, 1),
    )


def solution(mesh):
    return jax.shard_map(
        functools.partial(shards, mesh.shape["kv"]),
        mesh=mesh,
        in_specs=(
            P(("grp", "dp"), None, ("kv", "tp")),
            P(),
            P(None, "kv", None),
            P(None, "kv", None),
            P(None, "kv", "tp"),
            P(None, "kv", "tp"),
            P(),
            P(),
            P(),
            P(),
            P("kv", "tp", None),
            P(("grp", "dp"), "kv", "tp", None),
            P(("grp", "dp"), "kv", None),
            P(("grp", "dp"), "kv"),
            P(("grp", "dp"), None, "kv", None),
            P(("grp", "dp"), None, "kv", "tp"),
            P(("grp", "dp"), None, "kv"),
            P(("grp", "dp"), None, "kv"),
            P(("grp", "dp")),
        ),
        out_specs=(
            P(("grp", "dp"), None, ("kv", "tp")),
            P(("grp", "dp"), "kv", "tp", None),
            P(("grp", "dp"), "kv", None),
            P(("grp", "dp"), "kv"),
            P(("grp", "dp"), None, "kv", None),
            P(("grp", "dp"), None, "kv", "tp"),
            P(("grp", "dp"), None, "kv"),
            P(("grp", "dp"), None, "kv"),
        ),
        check_vma=False,
    )
```

time: 166 us -> 87.5 us (0.53)
  Pallas kernels: 0 us -> 77.9 us
  matrix products: 57.6 us -> 0 us
  local copies, waits for them, and re-layouts: 48.6 us -> 8.48 us
  other arithmetic: 34.2 us -> 0 us
  between operations: 14.6 us -> 0.7 us
  starting transfers between devices: 6.58 us -> 0 us
  blocking collectives: 2.62 us -> 0 us
    pallas_call x0 -> x3, Pallas kernels: none -> 77.9 us  [the longest x1 34.6 us: shards(): pl.pallas_call(functools.partial(output_kernel, n, values * 2), out_shape...]
    dot_general x13 -> x0, matrix products: 57.6 us -> none  [the longest x6 18.8 us: project(): jnp.dot(normed, weight.reshape(model_width, -1), preferred_element_type=j...]
    unnamed x1 -> x0, other arithmetic: 22.9 us -> none
    unnamed x80 -> x8, local copies, waits for them, and re-layouts: 21.5 us -> 0.02 us
    reshape x7, local copies, waits for them, and re-layouts: 17.8 us -> 7.01 us  [the longest x1 1.72 us: shards(): y.reshape(seqs, span, width)]
    all_to_all x1 -> x0, starting transfers between devices: 6.5 us -> none  [shards(): lax.all_to_all(w_out.reshape(1, local_heads * value_part, model_width), (...]
    convert_element_type x2 -> x0, other arithmetic: 5.06 us -> none  [shards(): normed = (as_float * inv_scale * norm_gain).astype(jnp.bfloat16)]
    all_to_all x1 -> x0, local copies, waits for them, and re-layouts: 3.98 us -> none  [shards(): lax.all_to_all(w_out.reshape(1, local_heads * value_part, model_width), (...]
  transfers between devices with their start and end apart: 3 -> 0, of which waited for: 0 -> 0; matrix products, arithmetic and copies ran while one was open for 81% -> 0% of each run, Pallas kernels for 0% -> 0%
where the time goes in v1:
time: 87.5 us; the launch traced here: 87.1 us
  Pallas kernels  77.9 us (89%)
  local copies, waits for them, and re-layouts  8.48 us (10%)
    pallas_call x1, Pallas kernels, shards(): pl.pallas_call(functools.partial(output_kernel, n, values * 2), out_shape...  34.6 us
    pallas_call x1, Pallas kernels, shards(): pl.pallas_call(functools.partial(project_kernel, n, keys), out_shape=[sds...  29.5 us
    pallas_call x1, Pallas kernels, shards(): pl.pallas_call(recurrent_kernel, grid=(seqs // block,), out_shape=[sds(me...  13.9 us

profile of v1, /device:TPU:0, one launch (start us, length us, event | category | flops | bytes accessed | tf_op | source)
XLA Modules:
  0.0 87.1 jit_solution(14482187629572729453)
XLA Ops:
  0.6 1.4 %dynamic_slice.3.gain_ref = f32[4,64]{1,0:T(4,128)} dynamic-slice(f32[16,128]{1,0:T(8,128)} %param.28, s32[]{:T(128)S(6)} %select_n.6, s32[]{:T(128)S(6)} %select_n.7), dynamic_slice_sizes={4,64} | dynamic-slice | bytes 2052 | tf_op jit(solution)/shard_map/dynamic_slice | solution.py:516
  2.0 1.7 %reshape.58.x_ref = bf16[256,512]{1,0:T(8,128)(2,1)} reshape(bf16[64,4,512]{2,1,0:T(4,128)(2,1)} %param.19) | data formatting | bytes 524288 | tf_op jit(solution)/shard_map/reshape | solution.py:511
  3.7 0.0 copy-start.2
  3.7 0.0 copy-start.3
  3.7 29.5 %project.1 = (bf16[256,256]{1,0:T(8,128)(2,1)}, bf16[256,256]{1,0:T(8,128)(2,1)}, bf16[256,256]{1,0:T(8,128)(2,1)}, f32[256,256]{1,0:T(8,128)}, f32[4,256]{1,0:T...) custom-call(bf16[256,512]{1,0:T(8,128)(2,1)} %reshape.58.x_ref, f32[1,4096]{1,0:T(1,128)} %bitcast.35, ...), custom_call_target="tpu_custom_call" | custom-call | tf_op jit(solution)/shard_map/project/pallas_call | solution.py:483
  33.2 0.0 copy-done.2
  33.2 0.2 reshape.67
  33.4 0.8 copy.29
  34.2 0.0 copy-done.3
  34.2 0.9 reshape.66.pk_ref
  35.0 13.9 %recurrent.1 = (f32[64,4,64,64]{3,2,1,0:T(8,128)}, f32[64,4,64]{2,1,0:T(4,128)}, f32[4,64]{1,0:T(4,128)}, f32[4,4,64]{2,1,0:T(4,128)}, f32[4,4,64]{2,1,0:T(4,128...) custom-call(bf16[256,256]{1,0:T(8,128)(2,1)} %get-tuple-element.22.q_ref, bf16[256,256]{1,0:T(8,128)(2,1)} %get-tuple-element.23.k_ref, ...), custom_call_target="tpu_custom_call" | custom-call | tf_op jit(solution)/shard_map/recurrent/pallas_call | solution.py:524
  48.9 0.0 copy-start.1
  48.9 0.0 copy-start
  48.9 34.6 %output.1 = bf16[256,512]{1,0:T(8,128)(2,1)} custom-call(bf16[256,256]{1,0:T(8,128)(2,1)} %get-tuple-element.28.g_ref, f32[4,256]{1,0:T(4,128)} %get-tuple-element.29.sq_ref, bf16[4,512,512]{2,1,0:T(8,128)(2,1)} %get-tuple-element.30.w_ref), custom_call_target="tpu_custom_call" | custom-call | tf_op jit(solution)/shard_map/output/pallas_call | solution.py:556
  83.5 1.7 %reshape.69 = bf16[64,4,512]{2,1,0:T(4,128)(2,1)} reshape(bf16[256,512]{1,0:T(8,128)(2,1)} %output.1) | data formatting | bytes 524288 | tf_op jit(solution)/shard_map/reshape | solution.py:577
  85.2 0.0 copy-done.1
  85.2 0.1 copy.30
  85.3 0.9 reshape.71
  86.2 0.0 copy-done
  86.2 0.9 reshape.70
Async XLA Ops:
  3.7 29.5 %copy-start.2 = (bf16[64,4,4,64]{3,2,1,0:T(4,128)(2,1)S(1)}, bf16[64,4,4,64]{3,2,1,0:T(4,128)(2,1)}, u32[]{:S(2)}) copy-start(bf16[64,4,4,64]{3,2,1,0:T(4,128)(2,1)} %param.34) | copy-start | bytes 393220
  3.7 30.4 %copy-start.3 = (bf16[64,4,4,64]{3,2,1,0:T(4,128)(2,1)S(1)}, bf16[64,4,4,64]{3,2,1,0:T(4,128)(2,1)}, u32[]{:S(2)}) copy-start(bf16[64,4,4,64]{3,2,1,0:T(4,128)(2,1)} %param.33) | copy-start | bytes 393220
  48.9 36.3 %copy-start.1 = (bf16[256,256]{1,0:T(8,128)(2,1)S(1)}, bf16[256,256]{1,0:T(8,128)(2,1)}, u32[]{:S(2)}) copy-start(bf16[256,256]{1,0:T(8,128)(2,1)} %get-tuple-element.24.v_ref) | copy-start | bytes 393220
  48.9 37.3 %copy-start = (bf16[256,256]{1,0:T(8,128)(2,1)S(1)}, bf16[256,256]{1,0:T(8,128)(2,1)}, u32[]{:S(2)}) copy-start(bf16[256,256]{1,0:T(8,128)(2,1)} %get-tuple-element.23.k_ref) | copy-start | bytes 393220

commit v2 on v1

--- a/solution.py
+++ b/solution.py
@@ -44,42 +44,54 @@
 
 
 def project_kernel(
-    n, key_size,
-    x_ref, gain_ref, wq_hbm, wk_hbm, wv_hbm, wo_hbm, wi_ref, wf_ref, bias_ref, out_hbm,
+    n, key_size, halves,
+    x_ref, gain_ref, wq_hbm, wk_hbm, wv_hbm, wo_hbm, wi_hbm, wf_hbm, bias_ref, out_hbm,
     q_out, k_out, v_out, og_out, gi_out, gf_out, wout_out,
-    xg, wq, wk, wv, wo, q_acc, k_acc, v_acc, o_acc, gi_acc, gf_acc, ssr_acc, ssc_acc,
-    load_sem, send_sem, recv_sem, wsend_sem, wrecv_sem,
+    xg, weights, acc, squares,
+    load_sem, own_sem, send_sem, recv_sem, wsend_sem, wrecv_sem,
 ):
     z = lax.axis_index("kv")
     c = lax.axis_index("tp")
-    width = x_ref.shape[1]
-    loads = [
-        pltpu.make_async_copy(src, dst, load_sem.at[i])
-        for i, (src, dst) in enumerate(((wq_hbm, wq), (wk_hbm, wk), (wv_hbm, wv), (wo_hbm, wo)))
-    ]
+    width = x_ref.shape[2]
+    rows = x_ref.shape[0] * x_ref.shape[1]
+    height = rows // halves
+    loads, spans, at = [], [], 0
+    for i, src in enumerate((wq_hbm, wk_hbm, wv_hbm, wo_hbm, wi_hbm, wf_hbm)):
+        size = src.shape[0]
+        spans.append(slice(at, at + size))
+        loads.append(
+            pltpu.make_async_copy(src, weights.at[pl.ds(at, size)], load_sem.at[i])
+        )
+        at += size
     for load in loads:
         load.start()
+    mine = 2 * z + c
+    flat = x_ref[...].reshape(rows, width)
+    for half in range(halves):
+        xg[mine, half] = flat[half * height : (half + 1) * height]
+    acc[...] = jnp.zeros_like(acc)
+    squares[...] = jnp.zeros_like(squares)
     enter(n, z, c)
-    mine = 2 * z + c
-
-    def hop(src, slot, way, target):
+
+    def hop(slot, half, way, target):
         return pltpu.make_async_remote_copy(
-            src_ref=src, dst_ref=xg.at[slot],
-            send_sem=send_sem.at[way, slot], recv_sem=recv_sem.at[slot],
+            src_ref=xg.at[slot, half], dst_ref=xg.at[slot, half],
+            send_sem=send_sem.at[way, slot, half], recv_sem=recv_sem.at[slot, half],
             device_id=target, device_id_type=MESH,
         )
 
     up, down, side = {"kv": z + 1}, {"kv": z - 1}, {"tp": 1 - c}
 
-    @pl.when(z < n - 1)
-    def _():
-        hop(x_ref, mine, 0, up).start()
-
-    @pl.when(z > 0)
-    def _():
-        hop(x_ref, mine, 1, down).start()
-
-    hop(x_ref, mine, 2, side).start()
+    for half in range(halves):
+        @pl.when(z < n - 1)
+        def _():
+            hop(mine, half, 0, up).start()
+
+        @pl.when(z > 0)
+        def _():
+            hop(mine, half, 1, down).start()
+
+        hop(mine, half, 2, side).start()
 
     rows_out = out_hbm.shape[0]
 
@@ -96,103 +108,93 @@
         col = pl.multiple_of((2 * i + c) * width, width)
         return pltpu.make_async_copy(
             out_hbm.at[:, pl.ds(col, width)], wout_out.at[i, pl.ds(0, rows_out)],
-            load_sem.at[4 + i],
+            own_sem.at[i],
         )
 
     for i in range(n):
         out_piece(i).start()
         own_piece(i).start()
-
-    for acc in (q_acc, k_acc, v_acc, o_acc, gi_acc, gf_acc, ssr_acc, ssc_acc):
-        acc[...] = jnp.zeros_like(acc)
     for load in loads:
         load.wait()
 
-    def process(src, slot):
+    def process(slot):
         cols = pl.ds(pl.multiple_of(slot * width, width), width)
-        x = src[...].astype(F32)
-        xs = (x * gain_ref[:, cols]).astype(BF16)
+        x = jnp.concatenate([xg[slot, half] for half in range(halves)], axis=0).astype(F32)
         square = x * x
-        high = square.astype(BF16)
-        low = (square - high.astype(F32)).astype(BF16)
-        ones_row = jnp.ones((8, width), BF16)
-        ones_col = jnp.ones((k_acc.shape[1], width), BF16)
-        ssr_acc[...] += nt(ones_row, high) + nt(ones_row, low)
-        ssc_acc[...] += nt(high, ones_col) + nt(low, ones_col)
-        q_acc[...] += nt(wq[:, cols], xs)
-        k_acc[...] += nt(xs, wk[:, cols])
-        v_acc[...] += nt(wv[:, cols], xs)
-        o_acc[...] += nt(wo[:, cols], xs)
-        gi_acc[...] += nt(wi_ref[:, cols], xs)
-        gf_acc[...] += nt(wf_ref[:, cols], xs)
-
-    process(x_ref, mine)
-
-    def partner_block(owner):
+        total = squares[...]
+        for i in range(width // 128):
+            total = total + square[:, i * 128 : (i + 1) * 128]
+        squares[...] = total
+        acc[...] += nt(weights[:, cols], (x * gain_ref[:, cols]).astype(BF16))
+
+    def process_owner(owner):
+        process(2 * owner + c)
         slot = 2 * owner + 1 - c
-        hop(x_ref, slot, 2, side).wait_recv()
-        process(xg.at[slot], slot)
-
-    partner_block(z)
+        for half in range(halves):
+            hop(slot, half, 2, side).wait_recv()
+        process(slot)
+
+    def forward(k, half):
+        @pl.when(z - k >= 0)
+        def _():
+            slot = 2 * (z - k) + c
+            hop(slot, half, 0, up).wait_recv()
+
+            @pl.when(z < n - 1)
+            def _():
+                hop(slot, half, 0, up).start()
+
+            hop(slot, half, 2, side).start()
+
+        @pl.when(z + k <= n - 1)
+        def _():
+            slot = 2 * (z + k) + c
+            hop(slot, half, 1, down).wait_recv()
+
+            @pl.when(z > 0)
+            def _():
+                hop(slot, half, 1, down).start()
+
+            hop(slot, half, 2, side).start()
 
     def step(k, carry):
-        @pl.when(z - k >= 0)
-        def _():
-            slot = 2 * (z - k) + c
-            hop(x_ref, slot, 0, up).wait_recv()
-
-            @pl.when(z < n - 1)
-            def _():
-                hop(xg.at[slot], slot, 0, up).start()
-
-            hop(xg.at[slot], slot, 2, side).start()
-
-        @pl.when(z + k <= n - 1)
-        def _():
-            slot = 2 * (z + k) + c
-            hop(x_ref, slot, 1, down).wait_recv()
-
-            @pl.when(z > 0)
-            def _():
-                hop(xg.at[slot], slot, 1, down).start()
-
-            hop(xg.at[slot], slot, 2, side).start()
-
-        @pl.when(z - k >= 0)
-        def _():
-            slot = 2 * (z - k) + c
-            process(xg.at[slot], slot)
-            partner_block(z - k)
-
-        @pl.when(z + k <= n - 1)
-        def _():
-            slot = 2 * (z + k) + c
-            process(xg.at[slot], slot)
-            partner_block(z + k)
+        for half in range(halves - 1):
+            forward(k, half)
+
+        @pl.when(z - (k - 1) >= 0)
+        def _():
+            process_owner(z - (k - 1))
+
+        forward(k, halves - 1)
+
+        @pl.when((z + k - 1 <= n - 1) & (k > 1))
+        def _():
+            process_owner(z + k - 1)
 
         return carry
 
-    lax.fori_loop(1, n, step, 0)
-
-    inv_row = lax.rsqrt(ssr_acc[0:1] / gain_ref.shape[1] + EPS)
-    inv_col = lax.rsqrt(ssc_acc[...] / gain_ref.shape[1] + EPS)
-    q_out[...] = ((q_acc[...] * inv_row).astype(BF16).astype(F32) * key_size ** (-0.5)).astype(BF16)
-    k_out[...] = (k_acc[...] * inv_col).astype(BF16)
-    v_out[...] = (v_acc[...] * inv_row).astype(BF16)
-    og_out[...] = o_acc[...] * inv_row
-    all_heads = gf_acc.shape[0]
+    lax.fori_loop(1, n + 1, step, 0)
+
+    depth = gain_ref.shape[1]
+    total = nt(jnp.ones((8, 128), F32), squares[...], HIGHEST)
+    inv = lax.rsqrt(total[0:1] / depth + EPS)
+    q, k, v, og, gi, gf = [acc[part, :] * inv for part in spans]
+    q_out[...] = (q.astype(BF16).astype(F32) * key_size ** (-0.5)).astype(BF16)
+    k_out[...] = k.T.astype(BF16)
+    v_out[...] = v.astype(BF16)
+    og_out[...] = og
+    all_heads = gf.shape[0]
     diagonal = lax.broadcasted_iota(jnp.int32, (all_heads, all_heads), 0) == (
         lax.broadcasted_iota(jnp.int32, (all_heads, all_heads), 1)
     )
-    shift = nn(jnp.where(diagonal, bias_ref[...], 0.0), jnp.ones(gf_acc.shape, F32), HIGHEST)
-    gi_acc[...] = gi_acc[...] * inv_row
-    raw = gf_acc[...] * inv_row + shift
-    gf_acc[...] = jnp.minimum(raw, 0.0) - jnp.log1p(jnp.exp(-jnp.abs(raw)))
+    shift = nn(jnp.where(diagonal, bias_ref[...], 0.0), jnp.ones(gf.shape, F32), HIGHEST)
+    raw = gf + shift
+    gf = jnp.minimum(raw, 0.0) - jnp.log1p(jnp.exp(-jnp.abs(raw)))
     local_heads = gi_out.shape[0]
-    for acc, out in ((gi_acc, gi_out), (gf_acc, gf_out)):
-        total = acc[:local_heads]
+    for values, out in ((gi, gi_out), (gf, gf_out)):
+        total = values[:local_heads]
         for i in range(1, n):
-            total = jnp.where(z == i, acc[i * local_heads : (i + 1) * local_heads], total)
+            total = jnp.where(z == i, values[i * local_heads : (i + 1) * local_heads], total)
         out[...] = total
 
     for i in range(n):
@@ -201,16 +203,16 @@
 
     def drain(i, carry):
         slot = 2 * i + c
-
-        @pl.when((i <= z) & (z < n - 1))
-        def _():
-            hop(x_ref, slot, 0, up).wait_send()
-
-        @pl.when((i >= z) & (z > 0))
-        def _():
-            hop(x_ref, slot, 1, down).wait_send()
-
-        hop(x_ref, slot, 2, side).wait_send()
+        for half in range(halves):
+            @pl.when((i <= z) & (z < n - 1))
+            def _():
+                hop(slot, half, 0, up).wait_send()
+
+            @pl.when((i >= z) & (z > 0))
+            def _():
+                hop(slot, half, 1, down).wait_send()
+
+            hop(slot, half, 2, side).wait_send()
         return carry
 
     lax.fori_loop(0, n, drain, 0)
@@ -316,6 +318,16 @@
         q = q_ref[...]
         owner = iota(q.shape, 0) // keys
 
+        z = lax.axis_index("kv")
+        gains = gain_ref[:, :values]
+        for i in range(1, gain_ref.shape[1] // values):
+            gains = jnp.where(
+                lax.axis_index("tp") == i, gain_ref[:, i * values : (i + 1) * values], gains
+            )
+        local = gains[:heads]
+        for i in range(1, gain_ref.shape[0] // heads):
+            local = jnp.where(z == i, gains[i * heads : (i + 1) * heads], local)
+
         def tile(w):
             w = jnp.concatenate([w] * (8 // span), axis=0)
             return jnp.broadcast_to(w[None], (rows // 8, 8, rows)).reshape(rows, rows)
@@ -336,16 +348,16 @@
             cell = top / jnp.maximum(jnp.abs(under), floor)
             sq_ref[h : h + 1, :] = jnp.sum(cell * cell, axis=0, keepdims=True)
             gain = nn(
-                jnp.where(eye, gain_ref[h : h + 1, :], 0.0), jnp.ones((values, rows), F32), HIGHEST
+                jnp.where(eye, local[h : h + 1, :], 0.0), jnp.ones((values, rows), F32), HIGHEST
             )
             g_ref[part, :] = (jax.nn.sigmoid(og_ref[part, :]) * cell * gain).astype(BF16)
 
 
 def output_kernel(
-    n, full_values,
+    n, full_values, halves,
     g_ref, sq_ref, w_ref,
     y_ref,
-    g_in, sq_in, both, from_low, from_high, to_high, to_low,
+    g_in, sq_in, both, from_low, from_high, to_high, to_low, total,
     side_send, side_recv, up_send, up_recv, down_send, down_recv,
 ):
     z = lax.axis_index("kv")
@@ -377,89 +389,91 @@
         )
         both[:, i * channels : (i + 1) * channels] = scaled.T.astype(BF16)
 
-    def partial(d):
-        return nn(both[...], w_ref[d])
-
-    def upward(d):
+    height = both.shape[0] // halves
+
+    def partial(d, half):
+        return nn(both[half * height : (half + 1) * height], w_ref[d])
+
+    def upward(d, half):
         return pltpu.make_async_remote_copy(
-            src_ref=to_high.at[d], dst_ref=from_low.at[d],
-            send_sem=up_send.at[d], recv_sem=up_recv.at[d],
+            src_ref=to_high.at[d, half], dst_ref=from_low.at[d, half],
+            send_sem=up_send.at[d, half], recv_sem=up_recv.at[d, half],
             device_id={"kv": z + 1}, device_id_type=MESH,
         )
 
-    def downward(d):
+    def downward(d, half):
         return pltpu.make_async_remote_copy(
-            src_ref=to_low.at[d], dst_ref=from_high.at[d],
-            send_sem=down_send.at[d], recv_sem=down_recv.at[d],
+            src_ref=to_low.at[d, half], dst_ref=from_high.at[d, half],
+            send_sem=down_send.at[d, half], recv_sem=down_recv.at[d, half],
             device_id={"kv": z - 1}, device_id_type=MESH,
         )
 
     def step(i, carry):
-        high = n - i
-        low = i - 1
-
-        @pl.when(high > z)
-        def _():
-            to_high[high] = partial(high).astype(BF16)
-
-            @pl.when(z > 0)
-            def _():
-                upward(high).wait_recv()
-                to_high[high] = (
-                    to_high[high].astype(F32) + from_low[high].astype(F32)
-                ).astype(BF16)
-
-            upward(high).start()
-
-        @pl.when(low < z)
-        def _():
-            to_low[low] = partial(low).astype(BF16)
-
-            @pl.when(z < n - 1)
-            def _():
-                downward(low).wait_recv()
-                to_low[low] = (
-                    to_low[low].astype(F32) + from_high[low].astype(F32)
-                ).astype(BF16)
-
-            downward(low).start()
+        high = n - 1 - i + z
+        low = i - (n - 1 - z)
+        for half in range(halves):
+            @pl.when((high > z) & (high <= n - 1))
+            def _():
+                term = partial(high, half)
+
+                @pl.when(z == 0)
+                def _():
+                    to_high[high, half] = term.astype(BF16)
+
+                @pl.when(z > 0)
+                def _():
+                    upward(high, half).wait_recv()
+                    to_high[high, half] = (term + from_low[high, half].astype(F32)).astype(BF16)
+
+                upward(high, half).start()
+
+            @pl.when((low < z) & (low >= 0))
+            def _():
+                term = partial(low, half)
+
+                @pl.when(z == n - 1)
+                def _():
+                    to_low[low, half] = term.astype(BF16)
+
+                @pl.when(z < n - 1)
+                def _():
+                    downward(low, half).wait_recv()
+                    to_low[low, half] = (term + from_high[low, half].astype(F32)).astype(BF16)
+
+                downward(low, half).start()
 
         return carry
 
-    lax.fori_loop(1, n, step, 0)
-    total = partial(z)
-    y_ref[...] = total.astype(BF16)
-
-    @pl.when(z == 0)
-    def _():
-        downward(z).wait_recv()
-        y_ref[...] = (partial(z) + from_high[z].astype(F32)).astype(BF16)
-
-    @pl.when(z == n - 1)
-    def _():
-        upward(z).wait_recv()
-        y_ref[...] = (partial(z) + from_low[z].astype(F32)).astype(BF16)
-
-    @pl.when((z > 0) & (z < n - 1))
-    def _():
-        upward(z).wait_recv()
-        downward(z).wait_recv()
-        y_ref[...] = (
-            partial(z) + from_low[z].astype(F32) + from_high[z].astype(F32)
-        ).astype(BF16)
+    lax.fori_loop(0, 2 * n - 2, step, 0)
+    for half in range(halves):
+        total[half] = partial(z, half)
+    for half in range(halves):
+        @pl.when(z > 0)
+        def _():
+            upward(z, half).wait_recv()
+            total[half] += from_low[z, half].astype(F32)
+
+        @pl.when(z < n - 1)
+        def _():
+            downward(z, half).wait_recv()
+            total[half] += from_high[z, half].astype(F32)
+
+    seqs, span, width = y_ref.shape
+    y_ref[...] = total[...].reshape(seqs, span, width).astype(BF16)
 
     def drain(i, carry):
-        @pl.when(n - i > z)
-        def _():
-            upward(n - i).wait_send()
-
-        @pl.when(i - 1 < z)
-        def _():
-            downward(i - 1).wait_send()
+        for half in range(halves):
+            @pl.when(i > z)
+            def _():
+                upward(i, half).wait_send()
+
+            @pl.when(i < z)
+            def _():
+                downward(i, half).wait_send()
 
         return carry
 
-    lax.fori_loop(1, n, drain, 0)
+    lax.fori_loop(0, n, drain, 0)
     for swap in swaps:
         swap.wait_send()
 
@@ -480,26 +494,27 @@
     hbm = pl.BlockSpec(memory_space=pl.ANY)
     flip = lambda w: w.transpose(1, 2, 0).reshape(-1, depth)
 
+    halves = 2
+    height = rows // halves
+    channels = 2 * hk + 2 * hv + 2 * all_heads
     q, k, v, og, gi, gf, wout = pl.pallas_call(
-        functools.partial(project_kernel, n, keys),
+        functools.partial(project_kernel, n, keys, halves),
         out_shape=[
             sds((hk, rows), BF16), sds((rows, hk), BF16), sds((hv, rows), BF16),
             sds((hv, rows), F32), sds((heads, rows), F32), sds((heads, rows), F32),
             sds((n, 2 * hv, width), BF16),
         ],
-        in_specs=[vm, vm, hbm, hbm, hbm, hbm, vm, vm, vm, hbm],
-        out_specs=[vm] * 6 + [vm],
+        in_specs=[vm, vm] + [hbm] * 6 + [vm, hbm],
+        out_specs=[vm] * 7,
         scratch_shapes=[
-            pltpu.VMEM((2 * n, rows, width), BF16),
-            pltpu.VMEM((hk, depth), BF16), pltpu.VMEM((hk, depth), BF16),
-            pltpu.VMEM((hv, depth), BF16), pltpu.VMEM((hv, depth), BF16),
-            pltpu.VMEM((hk, rows), F32), pltpu.VMEM((rows, hk), F32),
-            pltpu.VMEM((hv, rows), F32), pltpu.VMEM((hv, rows), F32),
-            pltpu.VMEM((all_heads, rows), F32), pltpu.VMEM((all_heads, rows), F32),
-            pltpu.VMEM((8, rows), F32), pltpu.VMEM((rows, hk), F32),
-            pltpu.SemaphoreType.DMA((4 + n,)),
-            pltpu.SemaphoreType.DMA((3, 2 * n)),
-            pltpu.SemaphoreType.DMA((2 * n,)),
+            pltpu.VMEM((2 * n, halves, height, width), BF16),
+            pltpu.VMEM((channels, depth), BF16),
+            pltpu.VMEM((channels, rows), F32),
+            pltpu.VMEM((rows, 128), F32),
+            pltpu.SemaphoreType.DMA((6,)),
+            pltpu.SemaphoreType.DMA((n,)),
+            pltpu.SemaphoreType.DMA((3, 2 * n, halves)),
+            pltpu.SemaphoreType.DMA((2 * n, halves)),
             pltpu.SemaphoreType.DMA((n,)),
             pltpu.SemaphoreType.DMA((n,)),
         ],
@@ -508,16 +523,11 @@
         ),
         name="project",
     )(
-        tokens.reshape(rows, width), norm_gain.reshape(1, depth),
+        tokens, norm_gain.reshape(1, depth),
         flip(w_query), flip(w_key), flip(w_value), flip(w_outgate),
         w_input.T, w_forget.T, forget_bias.reshape(1, all_heads), w_out.reshape(hv, -1),
     )
 
-    gain_block = lax.dynamic_slice(
-        head_gain,
-        (lax.axis_index("kv") * heads, lax.axis_index("tp") * values),
-        (heads, values),
-    )
     block = 8
     whole = lambda *shape: pl.BlockSpec(shape, lambda i: (0,) * len(shape))
     tile = pl.BlockSpec((block, heads, values, keys), lambda i: (i, 0, 0, 0))
@@ -533,7 +543,7 @@
             whole(hk, rows), whole(rows, hk), whole(hv, rows), whole(hv, rows),
             whole(heads, rows), whole(heads, rows), whole(rows, hk), whole(hv, rows),
             whole(span, heads, seqs), whole(span, heads, seqs), whole(1, seqs),
-            whole(heads, seqs), whole(seqs, heads, keys), whole(heads, values), tile,
+            whole(heads, seqs), whole(seqs, heads, keys), whole(*head_gain.shape), tile,
         ],
         out_specs=[
             tile, whole(seqs, heads, keys), whole(heads, seqs), whole(span, heads, seqs),
@@ -550,23 +560,20 @@
         q, k, v, og, gi, gf, prev_keys.reshape(rows, hk),
         prev_values.reshape(rows, hv).T,
         prev_input.transpose(1, 2, 0), prev_forget.transpose(1, 2, 0),
-        accepted.reshape(1, seqs), stabilizer.T, normalizer, gain_block, memory,
+        accepted.reshape(1, seqs), stabilizer.T, normalizer, head_gain, memory,
     )
 
     y = pl.pallas_call(
-        functools.partial(output_kernel, n, values * 2),
-        out_shape=sds((rows, width), BF16),
+        functools.partial(output_kernel, n, values * 2, halves),
+        out_shape=sds(tokens.shape, BF16),
         in_specs=[vm] * 3,
         out_specs=vm,
-        scratch_shapes=[
-            pltpu.VMEM((hv, rows), BF16), pltpu.VMEM((heads, rows), F32),
-            pltpu.VMEM((rows, 2 * hv), BF16),
-            pltpu.VMEM((n, rows, width), BF16), pltpu.VMEM((n, rows, width), BF16),
-            pltpu.VMEM((n, rows, width), BF16), pltpu.VMEM((n, rows, width), BF16),
-            pltpu.SemaphoreType.DMA((2,)), pltpu.SemaphoreType.DMA((2,)),
-            pltpu.SemaphoreType.DMA((n,)), pltpu.SemaphoreType.DMA((n,)),
-            pltpu.SemaphoreType.DMA((n,)), pltpu.SemaphoreType.DMA((n,)),
-        ],
+        scratch_shapes=[pltpu.VMEM((hv, rows), BF16), pltpu.VMEM((heads, rows), F32)]
+        + [pltpu.VMEM((rows, 2 * hv), BF16)]
+        + [pltpu.VMEM((n, halves, height, width), BF16)] * 4
+        + [pltpu.VMEM((halves, height, width), F32)]
+        + [pltpu.SemaphoreType.DMA((2,))] * 2
+        + [pltpu.SemaphoreType.DMA((n, halves))] * 4,
         compiler_params=pltpu.CompilerParams(
             collective_id=1, has_side_effects=True, vmem_limit_bytes=VMEM_LIMIT
         ),
@@ -574,7 +581,7 @@
     )(g, sq, wout)
 
     return (
-        y.reshape(seqs, span, width),
+        y,
         new_memory,
         new_normalizer,
         ns.T,

time: 87.5 us -> 72.1 us (0.82)
  Pallas kernels: 77.9 us -> 65.6 us
  local copies, waits for them, and re-layouts: 8.48 us -> 5.44 us
    pallas_call x2, Pallas kernels: 64 us -> 51.7 us  [the longest x1 29 us: shards(): pl.pallas_call(functools.partial(project_kernel, n, keys, halves), out_sh...]
    reshape x2 -> x0, local copies, waits for them, and re-layouts: 3.43 us -> none  [the longest x1 1.72 us: shards(): y.reshape(seqs, span, width)]
    unnamed x8 -> x9, local copies, waits for them, and re-layouts: 0.02 us -> 1.76 us
    dynamic_slice x1 -> x0, local copies, waits for them, and re-layouts: 1.35 us -> none  [shards(): lax.dynamic_slice(head_gain, (lax.axis_index('kv') * heads, lax.axis_inde...]
where the time goes in v2:
time: 72.1 us; the launch traced here: 71.7 us
  Pallas kernels  65.6 us (91%)
  local copies, waits for them, and re-layouts  5.44 us (8%)
    pallas_call x1, Pallas kernels, shards(): pl.pallas_call(functools.partial(project_kernel, n, keys, halves), out_sh...  29 us
    pallas_call x1, Pallas kernels, shards(): pl.pallas_call(functools.partial(output_kernel, n, values * 2, halves), o...  22.7 us
    pallas_call x1, Pallas kernels, shards(): pl.pallas_call(recurrent_kernel, grid=(seqs // block,), out_shape=[sds(me...  13.9 us
    unnamed x9, local copies, waits for them, and re-layouts  1.76 us

profile of v2, /device:TPU:0, one launch (start us, length us, event | category | flops | bytes accessed | tf_op | source)
XLA Modules:
  0.0 71.7 jit_solution(16629640855155145412)
XLA Ops:
  0.6 0.0 copy-start.2
  0.6 0.0 copy-start.3
  0.7 29.0 %project.1 = (bf16[256,256]{1,0:T(8,128)(2,1)}, bf16[256,256]{1,0:T(8,128)(2,1)}, bf16[256,256]{1,0:T(8,128)(2,1)}, f32[256,256]{1,0:T(8,128)}, f32[4,256]{1,0:T...) custom-call(bf16[64,4,512]{2,1,0:T(4,128)(2,1)} %x_ref.1, f32[1,4096]{1,0:T(1,128)} %bitcast.35, ...), custom_call_target="tpu_custom_call" | custom-call | tf_op jit(solution)/shard_map/project/pallas_call | solution.py:500
  29.6 0.0 copy-done.2
  29.6 0.2 reshape.60
  29.8 0.8 %copy.29 = bf16[256,256]{0,1:T(8,128)(2,1)} copy(bf16[256,256]{1,0:T(8,128)(2,1)S(1)} %reshape.60) | data formatting | bytes 262144 | tf_op jit(solution)/shard_map/reshape | solution.py:561
  30.6 0.0 copy-done.3
  30.6 0.9 %reshape.59.pk_ref = bf16[256,256]{1,0:T(8,128)(2,1)} reshape(bf16[64,4,4,64]{3,2,1,0:T(4,128)(2,1)S(1)} %copy-done.3) | data formatting | bytes 262144 | tf_op jit(solution)/shard_map/reshape | solution.py:560
  31.5 13.9 %recurrent.1 = (f32[64,4,64,64]{3,2,1,0:T(8,128)}, f32[64,4,64]{2,1,0:T(4,128)}, f32[4,64]{1,0:T(4,128)}, f32[4,4,64]{2,1,0:T(4,128)}, f32[4,4,64]{2,1,0:T(4,128...) custom-call(bf16[256,256]{1,0:T(8,128)(2,1)} %get-tuple-element.22.q_ref, bf16[256,256]{1,0:T(8,128)(2,1)} %get-tuple-element.23.k_ref, ...), custom_call_target="tpu_custom_call" | custom-call | tf_op jit(solution)/shard_map/recurrent/pallas_call | solution.py:534
  45.4 0.0 copy-start.1
  45.4 0.0 copy-start
  45.4 22.7 %output.1 = bf16[64,4,512]{2,1,0:T(4,128)(2,1)} custom-call(bf16[256,256]{1,0:T(8,128)(2,1)} %get-tuple-element.28.g_ref, f32[4,256]{1,0:T(4,128)} %get-tuple-element.29.sq_ref, bf16[4,512,512]{2,1,0:T(8,128)(2,1)} %get-tuple-element.30.w_ref), custom_call_target="tpu_custom_call" | custom-call | tf_op jit(solution)/shard_map/output/pallas_call | solution.py:566
  68.1 0.0 copy-done.1
  68.1 0.1 copy.30
  68.2 0.9 %reshape.63 = bf16[64,4,4,64]{3,2,1,0:T(4,128)(2,1)} reshape(bf16[256,256]{1,0:T(8,128)(2,1)S(1)} %copy.30) | data formatting | bytes 262144 | tf_op jit(solution)/shard_map/reshape | solution.py:589
  69.1 0.0 copy-done
  69.1 0.9 %reshape.62 = bf16[64,4,4,64]{3,2,1,0:T(4,128)(2,1)} reshape(bf16[256,256]{1,0:T(8,128)(2,1)S(1)} %copy-done) | data formatting | bytes 262144 | tf_op jit(solution)/shard_map/reshape | solution.py:588
  70.0 1.7 %copy.32 = bf16[64,4,512]{2,1,0:T(4,128)(2,1)} copy(bf16[64,4,512]{2,1,0:T(4,128)(2,1)} %output.1) | data formatting | bytes 524288
Async XLA Ops:
  0.6 29.0 %copy-start.2 = (bf16[64,4,4,64]{3,2,1,0:T(4,128)(2,1)S(1)}, bf16[64,4,4,64]{3,2,1,0:T(4,128)(2,1)}, u32[]{:S(2)}) copy-start(bf16[64,4,4,64]{3,2,1,0:T(4,128)(2,1)} %param.34) | copy-start | bytes 393220
  0.6 30.0 %copy-start.3 = (bf16[64,4,4,64]{3,2,1,0:T(4,128)(2,1)S(1)}, bf16[64,4,4,64]{3,2,1,0:T(4,128)(2,1)}, u32[]{:S(2)}) copy-start(bf16[64,4,4,64]{3,2,1,0:T(4,128)(2,1)} %param.33) | copy-start | bytes 393220
  45.4 22.7 %copy-start.1 = (bf16[256,256]{1,0:T(8,128)(2,1)S(1)}, bf16[256,256]{1,0:T(8,128)(2,1)}, u32[]{:S(2)}) copy-start(bf16[256,256]{1,0:T(8,128)(2,1)} %get-tuple-element.24.v_ref) | copy-start | bytes 393220
  45.4 23.7 %copy-start = (bf16[256,256]{1,0:T(8,128)(2,1)S(1)}, bf16[256,256]{1,0:T(8,128)(2,1)}, u32[]{:S(2)}) copy-start(bf16[256,256]{1,0:T(8,128)(2,1)} %get-tuple-element.23.k_ref) | copy-start | bytes 393220

commit v3 on v2

--- a/solution.py
+++ b/solution.py
@@ -45,10 +45,10 @@
 
 def project_kernel(
     n, key_size, halves,
-    x_ref, gain_ref, wq_hbm, wk_hbm, wv_hbm, wo_hbm, wi_hbm, wf_hbm, bias_ref, out_hbm,
-    q_out, k_out, v_out, og_out, gi_out, gf_out, wout_out,
+    x_ref, gain_ref, wq_hbm, wk_hbm, wv_hbm, wo_hbm, wi_hbm, wf_hbm, bias_ref, pk_ref, pv_ref, out_hbm,
+    q_out, k_out, v_out, og_out, gi_out, gf_out, pk_out, pv_out, wout_out,
     xg, weights, acc, squares,
-    load_sem, own_sem, send_sem, recv_sem, wsend_sem, wrecv_sem,
+    load_sem, send_sem, recv_sem, wsend_sem, wrecv_sem,
 ):
     z = lax.axis_index("kv")
     c = lax.axis_index("tp")
@@ -93,27 +93,24 @@
 
         hop(mine, half, 2, side).start()
 
-    rows_out = out_hbm.shape[0]
 
     def out_piece(i):
         col = pl.multiple_of((2 * i + 1 - c) * width, width)
         return pltpu.make_async_remote_copy(
             src_ref=out_hbm.at[:, pl.ds(col, width)],
-            dst_ref=wout_out.at[i, pl.ds(rows_out, rows_out)],
+            dst_ref=wout_out.at[i],
             send_sem=wsend_sem.at[i], recv_sem=wrecv_sem.at[i],
             device_id=side, device_id_type=MESH,
         )
 
-    def own_piece(i):
-        col = pl.multiple_of((2 * i + c) * width, width)
-        return pltpu.make_async_copy(
-            out_hbm.at[:, pl.ds(col, width)], wout_out.at[i, pl.ds(0, rows_out)],
-            own_sem.at[i],
-        )
-
     for i in range(n):
         out_piece(i).start()
-        own_piece(i).start()
+    heads, values = pv_ref.shape[2:]
+    old_keys = pk_ref[...].astype(F32).reshape(rows, heads, key_size)
+    old_values = pv_ref[...].astype(F32).reshape(rows, heads, values)
+    for h in range(heads):
+        pk_out[:, h * key_size : (h + 1) * key_size] = old_keys[:, h, :].astype(BF16)
+        pv_out[h * values : (h + 1) * values, :] = old_values[:, h, :].T.astype(BF16)
     for load in loads:
         load.wait()
 
@@ -198,7 +195,6 @@
         out[...] = total
 
     for i in range(n):
-        own_piece(i).wait()
         out_piece(i).wait()
 
     def drain(i, carry):
@@ -237,15 +233,22 @@
         spread = (iota((seqs, rows), 0) == iota((seqs, rows), 1) // span)
         expand = spread.astype(F32)
         lane_pos = iota((span, rows), 1) % span == iota((span, rows), 0)
-        eye = iota((seqs, seqs), 0) == iota((seqs, seqs), 1)
         dropped = iota((span, seqs), 0) >= acc_ref[...]
         ro[...] = jnp.zeros_like(ro)
+        single = [
+            jnp.where(lane_pos, ref[h : h + 1, :], 0.0)
+            for h in range(heads)
+            for ref in (gi_ref, gf_ref)
+        ]
+        compact = nt(jnp.concatenate(single, axis=0), expand, HIGHEST)
+        position = iota((2 * span, seqs), 0)
+        stack, decays = [], []
         for h in range(heads):
             stab = stab_ref[h : h + 1, :]
             f = jnp.where(dropped, 0.0, pf_ref[:, h, :])
             i = jnp.where(dropped, FAR_NEGATIVE, pi_ref[:, h, :])
-            new_i = nt(jnp.where(lane_pos, gi_ref[h : h + 1, :], 0.0), expand, HIGHEST)
-            new_f = nt(jnp.where(lane_pos, gf_ref[h : h + 1, :], 0.0), expand, HIGHEST)
+            new_i = compact[2 * h * span : (2 * h + 1) * span]
+            new_f = compact[(2 * h + 1) * span : (2 * h + 2) * span]
             ni_ref[:, h, :] = new_i
             nf_ref[:, h, :] = new_f
             total = []
@@ -260,31 +263,36 @@
             u = e - run_prev + i
             ns = jnp.maximum(e + stab, jnp.max(u, axis=0, keepdims=True))
             ns_ref[h : h + 1, :] = ns
-            decay = jnp.exp(e + stab - ns)
-            shares = jnp.exp(u - ns)
-            share_row = jnp.sum(
-                jnp.where(lane_pos, nn(shares, expand, HIGHEST), 0.0), axis=0, keepdims=True
-            )
-            kps[h] = pk_ref[:, h * keys : (h + 1) * keys]
-            part = slice(h * values, (h + 1) * values)
-            vts[part, :] = (pv_ref[part, :].astype(F32) * share_row).astype(BF16)
-            full = nn(jnp.where(eye, decay, 0.0), jnp.ones((seqs, keys), F32), HIGHEST)
-            dfull[h] = full
-            mixed = jnp.where(spread, share_row, 0.0).astype(BF16)
-            nn_ref[:, h, :] = full * nrm_ref[:, h, :] + nn(mixed, kps[h])
-            gathered = jnp.zeros((16, rows), F32)
-            position = iota((2 * span, seqs), 0)
+            decays.append(jnp.exp(e + stab - ns))
+            stack += [jnp.exp(u - ns), jnp.zeros((8 - span, seqs), F32)]
             for t in range(span):
                 latest = total[span + t]
                 d = jnp.where(position <= span + t, latest - run_all + in_all, FAR_NEGATIVE)
                 g = latest + stab
                 top = jnp.maximum(jnp.max(d, axis=0, keepdims=True), g)
                 pad = jnp.zeros((16 - 2 * span - 2, seqs), F32)
-                stack = jnp.concatenate(
-                    [jnp.exp(d - top), jnp.exp(g - top), jnp.exp(-top), pad], axis=0
+                stack += [jnp.exp(d - top), jnp.exp(g - top), jnp.exp(-top), pad]
+        wide = nn(jnp.concatenate(stack, axis=0), expand, HIGHEST)
+        decays = jnp.concatenate(decays + [jnp.zeros((8 - heads, seqs), F32)], axis=0).T
+        each = 8 + 16 * span
+        for h in range(heads):
+            base = h * each
+            share_row = jnp.sum(
+                jnp.where(lane_pos, wide[base : base + span], 0.0), axis=0, keepdims=True
+            )
+            kps[h] = pk_ref[:, h * keys : (h + 1) * keys]
+            part = slice(h * values, (h + 1) * values)
+            vts[part, :] = (pv_ref[part, :].astype(F32) * share_row).astype(BF16)
+            full = jnp.broadcast_to(decays[:, h : h + 1], (seqs, keys))
+            dfull[h] = full
+            mixed = jnp.where(spread, share_row, 0.0).astype(BF16)
+            nn_ref[:, h, :] = full * nrm_ref[:, h, :] + nn(mixed, kps[h])
+            gathered = jnp.zeros((16, rows), F32)
+            for t in range(span):
+                at = base + 8 + 16 * t
+                gathered = jnp.where(
+                    iota((16, rows), 1) % span == t, wide[at : at + 16], gathered
                 )
-                wide = nn(stack, expand, HIGHEST)
-                gathered = jnp.where(iota((16, rows), 1) % span == t, wide, gathered)
             wexp[h] = gathered
 
     first = step * block
@@ -314,7 +322,6 @@
     def _():
         same = iota((rows, rows), 0) // span == iota((rows, rows), 1) // span
         spread = iota((seqs, rows), 0) == iota((seqs, rows), 1) // span
-        eye = iota((values, values), 0) == iota((values, values), 1)
         q = q_ref[...]
         owner = iota(q.shape, 0) // keys
 
@@ -327,6 +334,8 @@
         local = gains[:heads]
         for i in range(1, gain_ref.shape[0] // heads):
             local = jnp.where(z == i, gains[i * heads : (i + 1) * heads], local)
+
+        columns = jnp.concatenate([local, jnp.zeros((8 - heads, values), F32)], axis=0).T
 
         def tile(w):
             w = jnp.concatenate([w] * (8 // span), axis=0)
@@ -347,21 +356,36 @@
             under = jnp.sum(w_prev + w_new, axis=0, keepdims=True) + carry * nq
             cell = top / jnp.maximum(jnp.abs(under), floor)
             sq_ref[h : h + 1, :] = jnp.sum(cell * cell, axis=0, keepdims=True)
-            gain = nn(
-                jnp.where(eye, local[h : h + 1, :], 0.0), jnp.ones((values, rows), F32), HIGHEST
-            )
+            gain = columns[:, h : h + 1]
             g_ref[part, :] = (jax.nn.sigmoid(og_ref[part, :]) * cell * gain).astype(BF16)
 
 
 def output_kernel(
     n, full_values, halves,
-    g_ref, sq_ref, w_ref,
+    g_ref, sq_ref, own_hbm, other_hbm,
     y_ref,
-    g_in, sq_in, both, from_low, from_high, to_high, to_low, total,
+    g_in, sq_in, both, from_low, from_high, to_high, to_low, total, w_ref,
+    load_sem,
     side_send, side_recv, up_send, up_recv, down_send, down_recv,
 ):
     z = lax.axis_index("kv")
     c = lax.axis_index("tp")
+    channels = g_ref.shape[0]
+    width = y_ref.shape[2]
+    loads = []
+    for d in range(n):
+        col = pl.multiple_of((2 * d + c) * width, width)
+        loads += [
+            pltpu.make_async_copy(
+                own_hbm.at[:, pl.ds(col, width)], w_ref.at[d, pl.ds(0, channels)],
+                load_sem.at[2 * d],
+            ),
+            pltpu.make_async_copy(
+                other_hbm.at[d], w_ref.at[d, pl.ds(channels, channels)], load_sem.at[2 * d + 1]
+            ),
+        ]
+    for load in loads:
+        load.start()
     enter(n, z, c)
     side = {"tp": 1 - c}
     swaps = [
@@ -376,7 +400,6 @@
     for swap in swaps:
         swap.wait_recv()
     inv = lax.rsqrt((sq_ref[...] + sq_in[...]) / full_values + EPS)
-    channels = g_ref.shape[0]
     heads = sq_ref.shape[0]
     values = channels // heads
     for i, src in enumerate((g_ref, g_in)):
@@ -389,6 +412,8 @@
         )
         both[:, i * channels : (i + 1) * channels] = scaled.T.astype(BF16)
 
+    for load in loads:
+        load.wait()
     height = both.shape[0] // halves
 
     def partial(d, half):
@@ -497,22 +522,21 @@
     halves = 2
     height = rows // halves
     channels = 2 * hk + 2 * hv + 2 * all_heads
-    q, k, v, og, gi, gf, wout = pl.pallas_call(
+    q, k, v, og, gi, gf, pk, pv, wout = pl.pallas_call(
         functools.partial(project_kernel, n, keys, halves),
         out_shape=[
             sds((hk, rows), BF16), sds((rows, hk), BF16), sds((hv, rows), BF16),
             sds((hv, rows), F32), sds((heads, rows), F32), sds((heads, rows), F32),
-            sds((n, 2 * hv, width), BF16),
+            sds((rows, hk), BF16), sds((hv, rows), BF16), sds((n, hv, width), BF16),
         ],
-        in_specs=[vm, vm] + [hbm] * 6 + [vm, hbm],
-        out_specs=[vm] * 7,
+        in_specs=[vm, vm] + [hbm] * 6 + [vm, vm, vm, hbm],
+        out_specs=[vm] * 8 + [hbm],
         scratch_shapes=[
             pltpu.VMEM((2 * n, halves, height, width), BF16),
             pltpu.VMEM((channels, depth), BF16),
             pltpu.VMEM((channels, rows), F32),
             pltpu.VMEM((rows, 128), F32),
             pltpu.SemaphoreType.DMA((6,)),
-            pltpu.SemaphoreType.DMA((n,)),
             pltpu.SemaphoreType.DMA((3, 2 * n, halves)),
             pltpu.SemaphoreType.DMA((2 * n, halves)),
             pltpu.SemaphoreType.DMA((n,)),
@@ -525,7 +549,8 @@
     )(
         tokens, norm_gain.reshape(1, depth),
         flip(w_query), flip(w_key), flip(w_value), flip(w_outgate),
-        w_input.T, w_forget.T, forget_bias.reshape(1, all_heads), w_out.reshape(hv, -1),
+        w_input.T, w_forget.T, forget_bias.reshape(1, all_heads), prev_keys, prev_values,
+        w_out.reshape(hv, -1),
     )
 
     block = 8
@@ -557,8 +582,7 @@
         compiler_params=pltpu.CompilerParams(vmem_limit_bytes=VMEM_LIMIT),
         name="recurrent",
     )(
-        q, k, v, og, gi, gf, prev_keys.reshape(rows, hk),
-        prev_values.reshape(rows, hv).T,
+        q, k, v, og, gi, gf, pk, pv,
         prev_input.transpose(1, 2, 0), prev_forget.transpose(1, 2, 0),
         accepted.reshape(1, seqs), stabilizer.T, normalizer, head_gain, memory,
     )
@@ -566,19 +590,20 @@
     y = pl.pallas_call(
         functools.partial(output_kernel, n, values * 2, halves),
         out_shape=sds(tokens.shape, BF16),
-        in_specs=[vm] * 3,
+        in_specs=[vm, vm, hbm, hbm],
         out_specs=vm,
         scratch_shapes=[pltpu.VMEM((hv, rows), BF16), pltpu.VMEM((heads, rows), F32)]
         + [pltpu.VMEM((rows, 2 * hv), BF16)]
         + [pltpu.VMEM((n, halves, height, width), BF16)] * 4
-        + [pltpu.VMEM((halves, height, width), F32)]
+        + [pltpu.VMEM((halves, height, width), F32), pltpu.VMEM((n, 2 * hv, width), BF16)]
+        + [pltpu.SemaphoreType.DMA((2 * n,))]
         + [pltpu.SemaphoreType.DMA((2,))] * 2
         + [pltpu.SemaphoreType.DMA((n, halves))] * 4,
         compiler_params=pltpu.CompilerParams(
             collective_id=1, has_side_effects=True, vmem_limit_bytes=VMEM_LIMIT
         ),
         name="output",
-    )(g, sq, wout)
+    )(g, sq, w_out.reshape(hv, -1), wout)
 
     return (
         y,

time: 72.1 us -> 68.1 us (0.945)
  Pallas kernels: 65.6 us -> 63.5 us
  local copies, waits for them, and re-layouts: 5.44 us -> 3.59 us
    reshape x3 -> x0, local copies, waits for them, and re-layouts: 1.84 us -> none  [the longest x2 0.97 us: shards(): prev_values.reshape(rows, hv)]
    pallas_call x1, Pallas kernels: 13.9 us -> 13.1 us  [shards(): pl.pallas_call(recurrent_kernel, grid=(seqs // block,), out_shape=[sds(me...]
    unnamed x9 -> x5, local copies, waits for them, and re-layouts: 1.76 us -> 1.75 us
where the time goes in v3:
time: 68.1 us; the launch traced here: 67.8 us
  Pallas kernels  63.5 us (93%)
  local copies, waits for them, and re-layouts  3.59 us (5%)
  between operations  0.69 us (1%)
    pallas_call x1, Pallas kernels, shards(): pl.pallas_call(functools.partial(project_kernel, n, keys, halves), out_sh...  28.4 us
    pallas_call x1, Pallas kernels, shards(): pl.pallas_call(functools.partial(output_kernel, n, values * 2, halves), o...  22 us
    pallas_call x1, Pallas kernels, shards(): pl.pallas_call(recurrent_kernel, grid=(seqs // block,), out_shape=[sds(me...  13.1 us
    unnamed x5, local copies, waits for them, and re-layouts  1.75 us

profile of v3, /device:TPU:0, one launch (start us, length us, event | category | flops | bytes accessed | tf_op | source)
XLA Modules:
  0.0 67.8 jit_solution(11898682141014681404)
XLA Ops:
  0.6 28.4 %project.1 = (bf16[256,256]{1,0:T(8,128)(2,1)}, bf16[256,256]{1,0:T(8,128)(2,1)}, bf16[256,256]{1,0:T(8,128)(2,1)}, f32[256,256]{1,0:T(8,128)}, f32[4,256]{1,0:T...) custom-call(bf16[64,4,512]{2,1,0:T(4,128)(2,1)} %x_ref.1, ...), custom_call_target="tpu_custom_call" | custom-call | tf_op jit(solution)/shard_map/project/pallas_call | solution.py:525
  29.1 13.1 %recurrent.1 = (f32[64,4,64,64]{3,2,1,0:T(8,128)}, f32[64,4,64]{2,1,0:T(4,128)}, f32[4,64]{1,0:T(4,128)}, f32[4,4,64]{2,1,0:T(4,128)}, f32[4,4,64]{2,1,0:T(4,128...) custom-call(bf16[256,256]{1,0:T(8,128)(2,1)} %get-tuple-element.24.q_ref, bf16[256,256]{1,0:T(8,128)(2,1)} %get-tuple-element.25.k_ref, ...), custom_call_target="tpu_custom_call" | custom-call | tf_op jit(solution)/shard_map/recurrent/pallas_call | solution.py:559
  42.1 0.0 copy-start.1
  42.1 0.0 copy-start
  42.1 22.0 %output.1 = bf16[64,4,512]{2,1,0:T(4,128)(2,1)} custom-call(bf16[256,256]{1,0:T(8,128)(2,1)} %get-tuple-element.32.g_ref, f32[4,256]{1,0:T(4,128)} %get-tuple-element.33.sq_ref, bf16[256,4096]{1,0:T(8,128)(2,1)} %bitcast.26, bf16[4,256,512]{2,1,0:T(8,128)(2,1)} %get-tuple-element.34.other_hbm), custom_call_target="tpu_custom_call" | custom-call | tf_op jit(solution)/shard_map/output/pallas_call | solution.py:590
  64.2 0.0 copy-done.1
  64.2 0.1 copy.28
  64.3 0.9 %reshape.56 = bf16[64,4,4,64]{3,2,1,0:T(4,128)(2,1)} reshape(bf16[256,256]{1,0:T(8,128)(2,1)S(1)} %copy.28) | data formatting | bytes 262144 | tf_op jit(solution)/shard_map/reshape | solution.py:614
  65.2 0.0 copy-done
  65.2 0.9 %reshape.55 = bf16[64,4,4,64]{3,2,1,0:T(4,128)(2,1)} reshape(bf16[256,256]{1,0:T(8,128)(2,1)S(1)} %copy-done) | data formatting | bytes 262144 | tf_op jit(solution)/shard_map/reshape | solution.py:613
  66.0 1.7 %copy.30 = bf16[64,4,512]{2,1,0:T(4,128)(2,1)} copy(bf16[64,4,512]{2,1,0:T(4,128)(2,1)} %output.1) | data formatting | bytes 524288
Async XLA Ops:
  42.1 22.1 %copy-start.1 = (bf16[256,256]{1,0:T(8,128)(2,1)S(1)}, bf16[256,256]{1,0:T(8,128)(2,1)}, u32[]{:S(2)}) copy-start(bf16[256,256]{1,0:T(8,128)(2,1)} %get-tuple-element.26.v_ref) | copy-start | bytes 393220
  42.1 23.0 %copy-start = (bf16[256,256]{1,0:T(8,128)(2,1)S(1)}, bf16[256,256]{1,0:T(8,128)(2,1)}, u32[]{:S(2)}) copy-start(bf16[256,256]{1,0:T(8,128)(2,1)} %get-tuple-element.25.k_ref) | copy-start | bytes 393220

commit v4 on v3

--- a/solution.py
+++ b/solution.py
@@ -280,13 +280,17 @@
             share_row = jnp.sum(
                 jnp.where(lane_pos, wide[base : base + span], 0.0), axis=0, keepdims=True
             )
-            kps[h] = pk_ref[:, h * keys : (h + 1) * keys]
+            old = pk_ref[:, h * keys : (h + 1) * keys]
+            odd = (iota((rows, keys), 0) // span) % 2
+            kps[h] = jnp.concatenate(
+                [jnp.where(odd == p, old, jnp.zeros_like(old)) for p in range(2)], axis=1
+            )
             part = slice(h * values, (h + 1) * values)
             vts[part, :] = (pv_ref[part, :].astype(F32) * share_row).astype(BF16)
             full = jnp.broadcast_to(decays[:, h : h + 1], (seqs, keys))
             dfull[h] = full
             mixed = jnp.where(spread, share_row, 0.0).astype(BF16)
-            nn_ref[:, h, :] = full * nrm_ref[:, h, :] + nn(mixed, kps[h])
+            nn_ref[:, h, :] = full * nrm_ref[:, h, :] + nn(mixed, old)
             gathered = jnp.zeros((16, rows), F32)
             for t in range(span):
                 at = base + 8 + 16 * t
@@ -298,24 +302,37 @@
     first = step * block
     start = pl.multiple_of((first * span) // lanes * lanes, lanes)
     half = pl.ds(start, lanes)
-    seq = (iota((values, lanes), 1) + start) // span - first
+    pair = ((iota((values, lanes), 1) + start) // span - first) // 2
+    parity = (iota((keys, lanes), 1) // span) % 2
     for h in range(heads):
         part = slice(h * values, (h + 1) * values)
         memory = [mem_ref[s, h] for s in range(block)]
-        packed = jnp.concatenate([m.astype(BF16) for m in memory], axis=0)
-        read = nn(packed, q_ref[h * keys : (h + 1) * keys, half])
+        packed = jnp.concatenate(
+            [
+                jnp.concatenate([memory[s].astype(BF16), memory[s + 1].astype(BF16)], axis=1)
+                for s in range(0, block, 2)
+            ],
+            axis=0,
+        )
+        query = q_ref[h * keys : (h + 1) * keys, half]
+        none = jnp.zeros_like(query)
+        both = jnp.concatenate([jnp.where(parity == p, query, none) for p in range(2)], axis=0)
+        read = nn(packed, both)
         total = ro[part, half]
-        for s in range(block):
-            total = jnp.where(seq == s, read[s * values : (s + 1) * values], total)
+        for s in range(block // 2):
+            total = jnp.where(pair == s, read[s * values : (s + 1) * values], total)
         ro[part, half] = total
         shared = vts[part, half]
         zero = jnp.zeros_like(shared)
-        left = jnp.concatenate([jnp.where(seq == s, shared, zero) for s in range(block)], axis=0)
+        left = jnp.concatenate(
+            [jnp.where(pair == s, shared, zero) for s in range(block // 2)], axis=0
+        )
         update = nn(left, kps[h, half, :])
         for s in range(block):
+            at = s // 2 * values
             nm_ref[s, h] = (
                 dfull[h, pl.ds(first + s, 1), :] * memory[s]
-                + update[s * values : (s + 1) * values]
+                + update[at : at + values, s % 2 * keys : (s % 2 + 1) * keys]
             )
 
     @pl.when(step == steps - 1)
@@ -575,7 +592,7 @@
             whole(span, heads, seqs), whole(hv, rows), whole(heads, rows),
         ],
         scratch_shapes=[
-            pltpu.VMEM((hv, rows), BF16), pltpu.VMEM((heads, rows, keys), BF16),
+            pltpu.VMEM((hv, rows), BF16), pltpu.VMEM((heads, rows, 2 * keys), BF16),
             pltpu.VMEM((heads, seqs, keys), F32), pltpu.VMEM((heads, 16, rows), F32),
             pltpu.VMEM((hv, rows), F32),
         ],

time: 68.1 us -> 67.8 us (level)
  no operation moved by 1% of the time
where the time goes in v4:
time: 67.8 us; the launch traced here: 67.5 us
  Pallas kernels  63.2 us (93%)
  local copies, waits for them, and re-layouts  3.59 us (5%)
  between operations  0.69 us (1%)
    pallas_call x1, Pallas kernels, shards(): pl.pallas_call(functools.partial(project_kernel, n, keys, halves), out_sh...  28.4 us
    pallas_call x1, Pallas kernels, shards(): pl.pallas_call(functools.partial(output_kernel, n, values * 2, halves), o...  22 us
    pallas_call x1, Pallas kernels, shards(): pl.pallas_call(recurrent_kernel, grid=(seqs // block,), out_shape=[sds(me...  12.7 us
    unnamed x5, local copies, waits for them, and re-layouts  1.75 us

profile of v4, /device:TPU:0, one launch (start us, length us, event | category | flops | bytes accessed | tf_op | source)
XLA Modules:
  0.0 67.5 jit_solution(14932283500795133297)
XLA Ops:
  0.6 28.4 %project.1 = (bf16[256,256]{1,0:T(8,128)(2,1)}, bf16[256,256]{1,0:T(8,128)(2,1)}, bf16[256,256]{1,0:T(8,128)(2,1)}, f32[256,256]{1,0:T(8,128)}, f32[4,256]{1,0:T...) custom-call(bf16[64,4,512]{2,1,0:T(4,128)(2,1)} %x_ref.1, ...), custom_call_target="tpu_custom_call" | custom-call | tf_op jit(solution)/shard_map/project/pallas_call | solution.py:542
  29.1 12.7 %recurrent.1 = (f32[64,4,64,64]{3,2,1,0:T(8,128)}, f32[64,4,64]{2,1,0:T(4,128)}, f32[4,64]{1,0:T(4,128)}, f32[4,4,64]{2,1,0:T(4,128)}, f32[4,4,64]{2,1,0:T(4,128...) custom-call(bf16[256,256]{1,0:T(8,128)(2,1)} %get-tuple-element.24.q_ref, bf16[256,256]{1,0:T(8,128)(2,1)} %get-tuple-element.25.k_ref, ...), custom_call_target="tpu_custom_call" | custom-call | tf_op jit(solution)/shard_map/recurrent/pallas_call | solution.py:576
  41.8 0.0 copy-start.1
  41.8 0.0 copy-start
  41.8 22.0 %output.1 = bf16[64,4,512]{2,1,0:T(4,128)(2,1)} custom-call(bf16[256,256]{1,0:T(8,128)(2,1)} %get-tuple-element.32.g_ref, f32[4,256]{1,0:T(4,128)} %get-tuple-element.33.sq_ref, bf16[256,4096]{1,0:T(8,128)(2,1)} %bitcast.26, bf16[4,256,512]{2,1,0:T(8,128)(2,1)} %get-tuple-element.34.other_hbm), custom_call_target="tpu_custom_call" | custom-call | tf_op jit(solution)/shard_map/output/pallas_call | solution.py:607
  63.9 0.0 copy-done.1
  63.9 0.1 copy.28
  64.0 0.9 %reshape.56 = bf16[64,4,4,64]{3,2,1,0:T(4,128)(2,1)} reshape(bf16[256,256]{1,0:T(8,128)(2,1)S(1)} %copy.28) | data formatting | bytes 262144 | tf_op jit(solution)/shard_map/reshape | solution.py:631
  64.8 0.0 copy-done
  64.8 0.9 %reshape.55 = bf16[64,4,4,64]{3,2,1,0:T(4,128)(2,1)} reshape(bf16[256,256]{1,0:T(8,128)(2,1)S(1)} %copy-done) | data formatting | bytes 262144 | tf_op jit(solution)/shard_map/reshape | solution.py:630
  65.7 1.7 %copy.30 = bf16[64,4,512]{2,1,0:T(4,128)(2,1)} copy(bf16[64,4,512]{2,1,0:T(4,128)(2,1)} %output.1) | data formatting | bytes 524288
Async XLA Ops:
  41.8 22.1 %copy-start.1 = (bf16[256,256]{1,0:T(8,128)(2,1)S(1)}, bf16[256,256]{1,0:T(8,128)(2,1)}, u32[]{:S(2)}) copy-start(bf16[256,256]{1,0:T(8,128)(2,1)} %get-tuple-element.26.v_ref) | copy-start | bytes 393220
  41.8 23.0 %copy-start = (bf16[256,256]{1,0:T(8,128)(2,1)S(1)}, bf16[256,256]{1,0:T(8,128)(2,1)}, u32[]{:S(2)}) copy-start(bf16[256,256]{1,0:T(8,128)(2,1)} %get-tuple-element.25.k_ref) | copy-start | bytes 393220
